TPU v7x, 256 devices: a whole 4x4x8 slice. The times are simulated.
256 devices in a mesh: sp: 16 (over y, x), tp: 16 (over z, core).
Axes of the slice: x: 4, y: 4, z: 8, core: 2. Of those that a mesh axis runs over, the one named last changes fastest.
Arguments:
- latent: bfloat16 [16384, 2048], P(('sp', 'tp')), may hold values from -1.5 to 1.5
- context: bfloat16 [512, 2048], P('sp'), may hold values from -6 to 6
- cond: bfloat16 [2048], replicated, may hold values from -6 to 6
- cond_context: bfloat16 [2048], replicated, may hold values from -6 to 6
- mod_weight: bfloat16 [3, 2048, 2048], P(None, 'sp', 'tp'), may hold values from -0.125 to 0.125
- norm_gain: bfloat16 [2048], replicated, may hold values from 0.099609375 to 1.8984375
- down_q: bfloat16 [2048, 768], P('tp'), may hold values from -0.125 to 0.125
- down_kv: bfloat16 [2048, 512], P('tp'), may hold values from -0.125 to 0.125
- rope_weight: bfloat16 [2048, 32], replicated, may hold values from -0.125 to 0.125
- qlat_gain: bfloat16 [768], replicated, may hold values from 0.099609375 to 1.8984375
- kvlat_gain: bfloat16 [512], replicated, may hold values from 0.099609375 to 1.8984375
- up_query: bfloat16 [768, 1536], P(None, 'tp'), may hold values from -0.21875 to 0.21875
- up_key: bfloat16 [512, 1024], P(None, 'tp'), may hold values from -0.25 to 0.25
- up_value: bfloat16 [512, 1024], P(None, 'tp'), may hold values from -0.25 to 0.25
- query_gain: float32 [96], replicated, may hold values from 0.5 to 8
- key_gain: float32 [96], replicated, may hold values from 0.5 to 8
- context_bias: float32 [16], P('tp'), may hold values from -2.2 to -0.7
- out_weight: bfloat16 [1024, 2048], P('tp'), may hold values from -48 to 48
Outputs:
- mixed: bfloat16 [16384, 2048], P(('sp', 'tp'))
All inputs are finite; a program needn't handle non-finite values.
Results may differ from a plain program's by a relative error of at most 0.028.
The roundings to bfloat16 on the way count: a program that leaves them out, or rounds other values in their place, can miss the bound.
Values may be sent and summed in bfloat16 or wider, within the bound.
A program may use at most 64 MiB of HBM per device.

v0:
```python
import functools
import math

import jax
import jax.numpy as jnp
from jax import lax
from jax.sharding import Mesh
from jax.sharding import PartitionSpec as P

NOPE = 64
ROPE = 32
VDIM = 64
GRID_W = 64
TOK_DEV = 1024
CTX_DEV = 32
SP = ("sp_0", "sp_1")
SP_TP = ("sp_0", "sp_1", "tp")


epsilon = 1e-06
theta = 10000.0


def over_axes(shard, axes):
    return functools.reduce(lax.psum, axes, shard)


def sent_together(arrays, axis, dim, along):
    ends, at = ([], 0)
    for a in arrays[:-1]:
        at += a.shape[along]
        ends.append(at)
    both = jnp.concatenate(arrays, axis=along)
    return tuple(jnp.split(lax.all_gather(both, axis, axis=dim, tiled=True), ends, axis=along))


def rms_scale(tensor, gain):
    return (
        tensor
        * lax.rsqrt(jnp.mean(tensor * tensor, axis=-1, keepdims=True) + epsilon)
        * gain.astype(jnp.float32)
    )


def axial_tables(positions):
    pair_count = ROPE // 4
    frequency = jnp.power(theta, -jnp.arange(pair_count, dtype=jnp.float32) / pair_count)
    row_angle = (positions // GRID_W).astype(jnp.float32)[:, None] * frequency
    col_angle = (positions % GRID_W).astype(jnp.float32)[:, None] * frequency
    return (jnp.cos(row_angle), jnp.sin(row_angle), jnp.cos(col_angle), jnp.sin(col_angle))


def rotate_half(tensor, cosine, sine_table):
    first, second = jnp.split(tensor, 2, axis=-1)
    cosine = cosine[:, None, :]
    sine_table = sine_table[:, None, :]
    return jnp.concatenate(
        [first * cosine - second * sine_table, second * cosine + first * sine_table], axis=-1
    )


def axial_rotate(tensor, tables):
    half_width = tensor.shape[-1] // 2
    return jnp.concatenate(
        [
            rotate_half(tensor[..., :half_width], tables[0], tables[1]),
            rotate_half(tensor[..., half_width:], tables[2], tables[3]),
        ],
        axis=-1,
    )


def modulate(row_block, gain, shifts, scales):
    normal = rms_scale(row_block.astype(jnp.float32), gain)
    return (normal * (1.0 + scales) + shifts).astype(jnp.bfloat16)


def make_queries(query_latent, up_query, query_gain, tables):
    amount = query_latent.shape[0]
    projected = jnp.dot(query_latent, up_query, preferred_element_type=jnp.float32).reshape(
        amount, -1, NOPE + ROPE
    )
    normal = rms_scale(projected, query_gain)
    return jnp.concatenate(
        [normal[..., :NOPE], axial_rotate(normal[..., NOPE:], tables)], axis=-1
    ).astype(jnp.bfloat16)


def make_keys(kv_latent, rope_rows, up_key, up_value, key_gain, tables):
    amount = kv_latent.shape[0]
    unrotated = jnp.dot(kv_latent, up_key, preferred_element_type=jnp.float32).reshape(
        amount, -1, NOPE
    )
    head_count = unrotated.shape[1]
    shared = rope_rows.astype(jnp.float32)[:, None, :]
    normal = rms_scale(jnp.concatenate([unrotated, shared], axis=-1), key_gain)
    if tables is not None:
        normal = jnp.concatenate(
            [normal[..., :NOPE], axial_rotate(normal[..., NOPE:], tables)], axis=-1
        )
    values = jnp.dot(kv_latent, up_value, preferred_element_type=jnp.float32).reshape(
        amount, head_count, VDIM
    )
    return (normal.astype(jnp.bfloat16), values.astype(jnp.bfloat16))


def absorb_block(state_in, queries, key_block, value_block, shift_heads):
    run_max, run_sum, run_acc = state_in
    scores = jnp.einsum("qhd,khd->qhk", queries, key_block, preferred_element_type=jnp.float32) * (
        NOPE + ROPE
    ) ** (-0.5)
    scores = scores + shift_heads[None, :, None]
    new_max = jnp.maximum(run_max, jnp.max(scores, axis=-1))
    factor = jnp.exp(run_max - new_max)
    weights = jnp.exp(scores - new_max[..., None])
    run_sum = run_sum * factor + jnp.sum(weights, axis=-1)
    run_acc = run_acc * factor[..., None] + jnp.einsum(
        "qhk,khd->qhd",
        weights.astype(jnp.bfloat16),
        value_block,
        preferred_element_type=jnp.float32,
    )
    return (new_max, run_sum, run_acc)


def shards(
    latent,
    context,
    cond,
    cond_context,
    mod_weight,
    norm_gain,
    down_q,
    down_kv,
    rope_weight,
    qlat_gain,
    kvlat_gain,
    up_query,
    up_key,
    up_value,
    query_gain,
    key_gain,
    context_bias,
    out_weight,
):
    seq_index = lax.axis_index(SP)
    tp_count = lax.axis_size("tp")
    own_rows = latent.shape[0]
    block_tokens = own_rows * tp_count
    row_span = mod_weight.shape[1]
    activated = jax.nn.silu(jnp.stack([cond, cond_context]).astype(jnp.float32)).astype(
        jnp.bfloat16
    )
    own_part = lax.dynamic_slice_in_dim(activated, seq_index * row_span, row_span, 1)
    partial_value = jnp.concatenate(
        [
            jnp.einsum("d,rde->re", own_part[0], mod_weight, preferred_element_type=jnp.float32),
            jnp.einsum(
                "d,rde->re", own_part[1], mod_weight[:2], preferred_element_type=jnp.float32
            ),
        ],
        axis=0,
    )
    summed = over_axes(partial_value, SP)
    modulations = lax.all_gather(summed, "tp", axis=1, tiled=True)
    normed = modulate(latent, norm_gain, modulations[0], modulations[1])
    context_normed = modulate(context, norm_gain, modulations[3], modulations[4])
    stacked = jnp.concatenate([normed, context_normed], axis=0)
    pieces = sent_together((down_q, down_kv), "tp", 0, 1)
    columns = stacked
    query_down = jnp.dot(columns[:own_rows], pieces[0], preferred_element_type=jnp.float32)
    kv_down = jnp.dot(columns, pieces[1], preferred_element_type=jnp.float32)
    query_latent = rms_scale(query_down, qlat_gain).astype(jnp.bfloat16)
    kv_latent = rms_scale(kv_down, kvlat_gain).astype(jnp.bfloat16)
    rope_rows = jnp.dot(stacked, rope_weight, preferred_element_type=jnp.float32).astype(
        jnp.bfloat16
    )
    all_query, all_kv, all_rope = sent_together(
        (query_latent, kv_latent[:own_rows], rope_rows[:own_rows]), "tp", 0, 1
    )
    own_context_keys, own_context_values = make_keys(
        kv_latent[own_rows:], rope_rows[own_rows:], up_key, up_value, key_gain, None
    )
    context_keys, context_values = sent_together((own_context_keys, own_context_values), SP, 0, 2)
    positions = seq_index * block_tokens + jnp.arange(block_tokens, dtype=jnp.int32)
    tables = axial_tables(positions)
    queries = make_queries(all_query, up_query, query_gain, tables)
    keys, values = make_keys(all_kv, all_rope, up_key, up_value, key_gain, tables)
    head_count = queries.shape[1]
    shift_heads = context_bias + math.log(TOK_DEV / CTX_DEV)
    start_state = (
        jnp.full((block_tokens, head_count), -jnp.inf, jnp.float32),
        jnp.zeros((block_tokens, head_count), jnp.float32),
        jnp.zeros((block_tokens, head_count, VDIM), jnp.float32),
    )
    state_now = absorb_block(start_state, queries, context_keys, context_values, shift_heads)
    no_shift = jnp.zeros((head_count,), jnp.float32)
    pieces = sent_together((keys, values), SP, 0, 2)
    amount = pieces[0].shape[0]
    span_rows = math.gcd(amount, 1024)
    key_blocks = pieces[0].reshape(amount // span_rows, span_rows, head_count, pieces[0].shape[2])
    value_blocks = pieces[1].reshape(amount // span_rows, span_rows, head_count, pieces[1].shape[2])

    def scan_step(state_mid, blocks):
        return (absorb_block(state_mid, queries, blocks[0], blocks[1], no_shift), None)

    state_out, unused = lax.scan(scan_step, state_now, (key_blocks, value_blocks))
    run_max, run_sum, run_acc = state_out
    attended = (
        (run_acc / run_sum[..., None]).astype(jnp.bfloat16).reshape(block_tokens, head_count * VDIM)
    )
    token_rows = lax.all_to_all(attended, "tp", split_axis=0, concat_axis=1, tiled=True)
    columns = token_rows
    projected = jnp.dot(
        columns,
        lax.all_gather(out_weight, "tp", axis=0, tiled=True),
        preferred_element_type=jnp.float32,
    )
    return (latent.astype(jnp.float32) + modulations[2] * projected).astype(jnp.bfloat16)


def solution(mesh):
    split = Mesh(mesh.devices.reshape(4, 4, mesh.shape["tp"]), ("sp_0", "sp_1", "tp"))
    placed = (
        P(SP_TP, None),
        P(SP, None),
        P(),
        P(),
        P(None, SP, "tp"),
        P(),
        P("tp", None),
        P("tp", None),
        P(),
        P(),
        P(),
        P(None, "tp"),
        P(None, "tp"),
        P(None, "tp"),
        P(),
        P(),
        P("tp"),
        P("tp", None),
    )
    return jax.shard_map(
        shards, mesh=split, in_specs=placed, out_specs=P(SP_TP, None), check_vma=False
    )
```

profile of v0, /device:TPU:1, one launch (start us, length us, event | category | flops | bytes accessed | tf_op | source)
XLA Modules:
  0.0 257.2 jit_solution(4174286790075011879)
XLA Ops:
  6.5 1.8 pad_maximum_fusion.2
  12.5 9.5 %psum.14 = f32[5,128]{1,0:T(8,128)S(1)} all-reduce(f32[5,128]{1,0:T(8,128)S(1)} %pad_maximum_fusion.8), channel_id=1, replica_groups=mesh['sp_0'=4,'sp_1'=4,'tp'=16] {'sp_0'}, use_global_device_ids=true, to_apply=%region_0.1 | all-reduce | flops 640 | bytes 5120 | tf_op jit(solution)/shard_map/psum | solution.py:25
  22.1 8.9 %psum.15 = f32[5,128]{1,0:T(8,128)S(1)} all-reduce(f32[5,128]{1,0:T(8,128)S(1)} %psum.14), channel_id=1, replica_groups=mesh['sp_0'=4,'sp_1'=4,'tp'=16] {'sp_1'}, use_global_device_ids=true, to_apply=%region_1.2 | all-reduce | flops 640 | bytes 5120 | tf_op jit(solution)/shard_map/psum | solution.py:25
  30.9 24.3 %all_gather.18 = f32[5,2048]{1,0:T(8,128)S(1)} all-gather(f32[5,128]{1,0:T(8,128)S(1)} %psum.15), channel_id=1, replica_groups=mesh['sp_0'=4,'sp_1'=4,'tp'=16] {'tp'}, dimensions={1}, use_global_device_ids=true | all-gather | bytes 43520 | tf_op jit(solution)/shard_map/all_gather | solution.py:165
  60.9 2.2 multiply_reduce_fusion.4
  63.2 2.6 %multiply_reduce_fusion.3 = (f32[64]{0:T(128)S(1)}, f32[64,768]{1,0:T(8,128)S(1)}) fusion(bf16[64,2048]{1,0:T(8,128)(2,1)S(1)} %fusion.49, bf16[2048,1280]{1,0:T(8,128)(2,1)} %all-gather.5.cloned.1.call-done), kind=kOutput, calls=%fused_computation.81 | convolution fusion | flops 201424832 | bytes 3604736 | tf_op jit(solution)/shard_map/dot_general | solution.py:171
  66.8 34.7 %all-gather.7.cloned.1.call-done = bf16[1024,1312]{1,0:T(8,128)(2,1)} async-done(((bf16[64,1312]{1,0:T(8,128)(2,1)}), bf16[1024,1312]{1,0:T(8,128)(2,1)}) %all-gather.7.cloned.1.call-update) | async-done | bytes 2686992 | tf_op jit(solution)/shard_map/all_gather | solution.py:34
  101.5 2.0 multiply_reduce_fusion.2
  107.7 1.7 fusion.36
  112.0 19.7 %all_gather.20 = bf16[512,1,160]{2,0,1:T(8,128)(2,1)S(1)} all-gather(bf16[32,1,160]{2,0,1:T(8,128)(2,1)S(1)} %pad_maximum_fusion.7), channel_id=1, replica_groups=mesh['sp_0'=4,'sp_1'=4,'tp'=16] {'sp_0','sp_1'}, dimensions={0}, use_global_device_ids=true | all-gather | bytes 174080 | tf_op jit(solution)/shard_map/all_gather | solution.py:34
  133.5 36.4 %all-gather.9.cloned.1.call-done = bf16[16384,1,160]{0,2,1:T(8,128)(2,1)} async-done(((bf16[1024,1,160]{0,2,1:T(8,128)(2,1)}), bf16[16384,1,160]{0,2,1:T(8,128)(2,1)}) %all-gather.9.cloned.1.call-update) | async-done | bytes 5242896 | tf_op jit(solution)/shard_map/all_gather | solution.py:34
  169.9 1.9 slice-done
  171.8 2.1 copy.43
  175.6 53.7 %while.14 = (s32[]{:T(128)}, f32[1024,1]{0,1:T(1,128)S(1)}, f32[1024,1]{0,1:T(1,128)S(1)}, f32[1024,1,64]{0,2,1:T(8,128)S(1)}, bf16[16,1024,1,96]{1,3,2,0:T(8,12...) while((s32[]{:T(128)}, f32[1024,1]{0,1:T(1,128)S(1)}, ...), condition=%wide.region_14.15_spmd, body=%wide.region_11.14_spmd.sunk | while | flops 344066048 | bytes 13697125 | solution.py:207
  175.6 1.7 multiply_reduce_fusion.7
  179.0 1.7 multiply_reduce_fusion.7
  182.3 1.7 multiply_reduce_fusion.7
  185.7 1.7 multiply_reduce_fusion.7
  189.0 1.7 multiply_reduce_fusion.7
  192.4 1.7 multiply_reduce_fusion.7
  195.7 1.7 multiply_reduce_fusion.7
  199.1 1.7 multiply_reduce_fusion.7
  202.5 1.7 multiply_reduce_fusion.7
  205.8 1.7 multiply_reduce_fusion.7
  209.2 1.7 multiply_reduce_fusion.7
  212.5 1.7 multiply_reduce_fusion.7
  215.9 1.7 multiply_reduce_fusion.7
  219.3 1.7 multiply_reduce_fusion.7
  222.6 1.7 multiply_reduce_fusion.7
  226.0 1.7 multiply_reduce_fusion.7
  229.8 16.6 %all_to_all.19 = bf16[16,2,2048]{2,1,0:T(2,128)(2,1)S(1)} all-to-all(bf16[16,2,2048]{2,1,0:T(2,128)(2,1)S(1)} %reshape.779), channel_id=1, replica_groups=mesh['sp_0'=4,'sp_1'=4,'tp'=16] {'tp'}, dimensions={0} | all-to-all | bytes 262144 | tf_op jit(solution)/shard_map/all_to_all | solution.py:212
  247.0 3.8 %fusion.24 = bf16[64,2048]{1,0:T(8,128)(2,1)} fusion(bf16[64,1024]{1,0:T(8,128)(2,1)S(1)} %all_to_all.17, bf16[1024,2048]{1,0:T(8,128)(2,1)} %all-gather.11.cloned.1.call-done, bf16[64,2048]{1,0:T(8,128)(2,1)S(1)} %copy-done.1, f32[2048]{0:T(1024)S(1)} %bitcast.194), kind=kOutput, calls=%fused_computation.25 | convolution fusion | flops 268959744 | bytes 4857856 | tf_op jit(solution)/shard_map/dot_general | solution.py:214
  (179 shorter events, 47.6 us)
Async XLA Ops:
  6.5 95.0 %copy-start = (bf16[768,96]{0,1:T(8,128)(2,1)S(1)}, bf16[768,96]{0,1:T(8,128)(2,1)}, u32[]{:S(2)}) copy-start(bf16[768,96]{0,1:T(8,128)(2,1)} %param.31) | copy-start | bytes 442372
  6.5 54.3 %copy-start.7 = (bf16[512]{0:T(512)(128)(2,1)S(1)}, bf16[512]{0:T(512)(128)(2,1)}, u32[]{:S(2)}) copy-start(bf16[512]{0:T(512)(128)(2,1)} %param.30) | copy-start | bytes 3076
  6.5 54.3 %copy-start.5 = (bf16[768]{0:T(1024)(128)(2,1)S(1)}, bf16[768]{0:T(1024)(128)(2,1)}, u32[]{:S(2)}) copy-start(bf16[768]{0:T(1024)(128)(2,1)} %param.29) | copy-start | bytes 4612
  6.5 54.4 %all-gather.5.cloned.1.call-start = ((), (), s32[]{:S(2)}) async-start(), calls=%async_computation.1 | async-start | bytes 5570560 | tf_op jit(solution)/shard_map/all_gather | solution.py:34
  8.3 93.2 %all-gather.7.cloned.1.call-start = ((), (), s32[]{:S(2)}) async-start(), calls=%async_computation.2 | async-start | bytes 3063808 | tf_op jit(solution)/shard_map/all_gather | solution.py:34
  63.2 40.4 %copy-start.8 = (f32[96]{0:T(128)S(1)}, f32[96]{0:T(128)}, u32[]{:S(2)}) copy-start(f32[96]{0:T(128)} %param.34) | copy-start | bytes 1156
  66.0 38.9 %copy-start.3 = (bf16[512,64]{0,1:T(8,128)(2,1)S(1)}, bf16[512,64]{0,1:T(8,128)(2,1)}, u32[]{:S(2)}) copy-start(bf16[512,64]{0,1:T(8,128)(2,1)} %param.32) | copy-start | bytes 196612
  66.7 103.2 %all-gather.9.cloned.1.call-start = ((), (), s32[]{:S(2)}) async-start(), calls=%async_computation.3 | async-start | bytes 5570560 | tf_op jit(solution)/shard_map/all_gather | solution.py:34
  66.8 39.8 %copy-start.6 = (f32[96]{0:T(128)S(1)}, f32[96]{0:T(128)}, u32[]{:S(2)}) copy-start(f32[96]{0:T(128)} %param.35) | copy-start | bytes 1156
  103.6 4.1 %copy-start.4 = (bf16[512,64]{0,1:T(8,128)(2,1)S(1)}, bf16[512,64]{0,1:T(8,128)(2,1)}, u32[]{:S(2)}) copy-start(bf16[512,64]{0,1:T(8,128)(2,1)} %param.33) | copy-start | bytes 196612
  109.4 0.7 copy-start.2
  110.1 136.8 %all-gather.11.cloned.1.call-start = ((), (), s32[]{:S(2)}) async-start(), calls=%async_computation.4 | async-start | bytes 4456448 | tf_op jit(solution)/shard_map/all_gather | solution.py:216
  169.9 1.9 slice-start
  173.8 1.6 slice-start.1
  229.3 17.7 %copy-start.1 = (bf16[64,2048]{1,0:T(8,128)(2,1)S(1)}, bf16[64,2048]{1,0:T(8,128)(2,1)}, u32[]{:S(2)}) copy-start(bf16[64,2048]{1,0:T(8,128)(2,1)} %param.20) | copy-start | bytes 786436
Sparse Core Ops, SparseCore 0:
  9.2 47.4 all-gather.4
  66.8 34.6 all-gather.6
  110.2 59.5 all-gather.8
  171.5 42.2 all-gather.10
where the time goes:
time: 258 us; the launch traced here: 257 us
  blocking collectives  79 us (31%)
  waiting for transfers between devices  71.7 us (28%)
  matrix products  59.1 us (23%)
  other arithmetic  23.2 us (9%)
  between operations  14.2 us (6%)
  local copies, waits for them, and re-layouts  9.15 us (4%)
    all_gather x3, waiting for transfers between devices, sent_together(): lax.all_gather(both, axis, axis=dim, tiled=True)  71.1 us
    dot_general x17, matrix products, absorb_block(): jnp.einsum('qhd,khd->qhk', queries, key_block, preferred_element_type=jnp...  27.1 us
    all_gather x1, blocking collectives, shards(): modulations = lax.all_gather(summed, 'tp', axis=1, tiled=True)  24.3 us
    all_gather x1, blocking collectives, sent_together(): lax.all_gather(both, axis, axis=dim, tiled=True)  19.7 us
    psum x2, blocking collectives, over_axes(): return functools.reduce(lax.psum, axes, shard)  18.4 us
    all_to_all x1, blocking collectives, shards(): lax.all_to_all(attended, 'tp', split_axis=0, concat_axis=1, tiled=True)  16.6 us
    dot_general x17, matrix products, absorb_block(): jnp.einsum('qhk,khd->qhd', weights.astype(jnp.bfloat16), value_block, pre...  14.7 us
    reduce_sum x17, other arithmetic, absorb_block(): run_sum = run_sum * factor + jnp.sum(weights, axis=-1)  12.1 us
  transfers between devices with their start and end apart: 4, of which 2 were waited for; matrix products, arithmetic and copies ran while one was open for 26% of the time, Pallas kernels for 0%

commit v1 on v0

v1 whole, which is shorter than its diff:
```python
import functools
import math

import jax
import jax.numpy as jnp
from jax import lax
from jax.experimental import pallas as pl
from jax.experimental.pallas import tpu as pltpu
from jax.sharding import PartitionSpec as P

NOPE = 64
ROPE = 32
HEAD = NOPE + ROPE
VDIM = 64
GRID_W = 64
TOK_DEV = 1024
CTX_DEV = 32
D = 2048
SP_TP = ("sp", "tp")
BF = jnp.bfloat16
F32 = jnp.float32

epsilon = 1e-06
theta = 10000.0
SCALE2 = math.log2(math.e) * HEAD ** (-0.5)
LOG2E = math.log2(math.e)


def exchange_items():
    items = {}
    for h in (0, 1):
        def add(da, db, part, axis, step, trigger):
            names = ("x", "y") if h == 0 else ("y", "x")
            items[(h, da, db, part)] = (names[axis], step, trigger)
        add(-1, 0, "U", 0, 1, None)
        add(1, 0, "U", 0, -1, None)
        add(2, 0, 0, 0, 1, (h, -1, 0, "U"))
        add(2, 0, 1, 0, -1, (h, 1, 0, "U"))
        for da in (0, -1, 1):
            trigger = None if da == 0 else (h, da, 0, "U")
            add(da, -1, "U", 1, 1, trigger)
            add(da, 1, "U", 1, -1, trigger)
            add(da, 2, 0, 1, 1, (h, da, -1, "U"))
            add(da, 2, 1, 1, -1, (h, da, 1, "U"))
        for q in (0, 1):
            add(2, -1, q, 1, 1, (h, 2, 0, q))
            add(2, 1, q, 1, -1, (h, 2, 0, q))
        add(2, 2, 0, 1, 1, (h, 2, -1, 0))
        add(2, 2, 1, 1, -1, (h, 2, 1, 1))
    return items


def arrival_times(items, unit=3.53, latency=1.8):
    free, arrive = {}, {}
    waiting = []
    for n, (key, (axis, step, trigger)) in enumerate(items.items()):
        if trigger is None:
            first = axis == ("x" if key[0] == 0 else "y")
            waiting.append((0.0, 0 if first else 1, n, key))
    count = len(items)
    while waiting:
        waiting.sort()
        at, _, _, key = waiting.pop(0)
        axis, step, _ = items[key]
        span = unit if key[3] == "U" else unit / 2
        begin = max(at, free.get((axis, step), 0.0))
        free[(axis, step)] = begin + span
        arrive[key] = begin + span + latency
        for other, (_, _, trigger) in items.items():
            if trigger == key:
                count += 1
                waiting.append((arrive[key], 0, count, other))
    return arrive


ITEMS = exchange_items()
ARRIVE = arrival_times(ITEMS)
ITEM_ORDER = sorted(ITEMS, key=lambda k: (round(ARRIVE[k], 1), str(k)))
ITEM_INDEX = {k: n for n, k in enumerate(ITEM_ORDER)}


def unit_order():
    ready = {}
    for k in ITEM_ORDER:
        ready[k[:3]] = max(ready.get(k[:3], 0.0), ARRIVE[k])
    units = sorted(ready, key=lambda u: (round(ready[u], 1), str(u)))
    return [(0, 0, 0), (1, 0, 0)] + units


UNITS = unit_order()
SLOT = {u: n for n, u in enumerate(UNITS)}
N_UNITS = len(UNITS) + 1
CTX_SLOT = len(UNITS)


def item_steps(per_step=0.62):
    steps = {}
    now = 0.0
    placed = set()
    plan = []
    for n in range(N_UNITS):
        need = []
        if n < len(UNITS):
            need = [k for k in ITEM_ORDER if k[:3] == UNITS[n] and k not in placed]
        for k in need:
            now = max(now, ARRIVE[k])
        early = [k for k in ITEM_ORDER if k not in placed and (k in need or ARRIVE[k] <= now)]
        placed.update(early)
        plan.append(early)
        now += per_step
    return plan


PLAN = item_steps()


class Board:
    def __init__(self, sends, recvs):
        self.sends, self.recvs, self.count, self.started = sends, recvs, 0, []

    def take(self, n=1):
        first = self.count
        self.count += n
        return first

    def send(self, number, src, dst, device):
        copy = pltpu.make_async_remote_copy(
            src_ref=src, dst_ref=dst, send_sem=self.sends.at[number],
            recv_sem=self.recvs.at[number], device_id=device,
            device_id_type=pl.DeviceIdType.MESH)
        copy.start()

    def arrived(self, number, dst, device):
        pltpu.make_async_remote_copy(
            src_ref=dst, dst_ref=dst, send_sem=self.sends.at[number],
            recv_sem=self.recvs.at[number], device_id=device,
            device_id_type=pl.DeviceIdType.MESH).wait_recv()

    def sent(self, number, src, device):
        pltpu.make_async_remote_copy(
            src_ref=src, dst_ref=src, send_sem=self.sends.at[number],
            recv_sem=self.recvs.at[number], device_id=device,
            device_id_type=pl.DeviceIdType.MESH).wait_send()


class Place:
    def __init__(self):
        self.s = lax.axis_index("sp")
        self.t = lax.axis_index("tp")
        self.y, self.x = self.s // 4, self.s % 4
        self.z, self.c = self.t // 2, self.t % 2

    def plane(self, axis, step):
        y, x = self.y, self.x
        if axis == "x":
            x = (x + step + 4) % 4
        else:
            y = (y + step + 4) % 4
        return {"sp": y * 4 + x, "tp": self.t}

    def sp_peer(self, k):
        return {"sp": (self.s + k) % 16, "tp": self.t}

    def tp_peer(self, k):
        return {"sp": self.s, "tp": (self.t + k) % 16}

    def ring(self, step):
        return {"sp": self.s, "tp": ((self.z + step + 8) % 8) * 2 + self.c}

    def sibling(self):
        return {"sp": self.s, "tp": self.z * 2 + 1 - self.c}


def greet(devices):
    barrier = pltpu.get_barrier_semaphore()
    for device in devices:
        pl.semaphore_signal(barrier, inc=1, device_id=device,
                            device_id_type=pl.DeviceIdType.MESH)
    pl.semaphore_wait(barrier, len(devices))


class ZRing:
    def __init__(self, board, place, own, bufs):
        self.board, self.place, self.own, self.bufs = board, place, own, bufs
        self.base = board.take(16)

    def number(self, way, dist, part):
        return self.base + (0 if way == 1 else 8) + (dist - 1) * 2 + part

    def slot(self, way, dist, part):
        return self.bufs[part].at[(self.place.z - way * dist + 16) % 8]

    def begin(self):
        for part in (0, 1):
            for way in (1, -1):
                self.board.send(self.number(way, 1, part), self.own[part],
                                self.bufs[part].at[self.place.z], self.place.ring(way))

    def take(self, way, dist, part):
        here = self.slot(way, dist, part)
        self.board.arrived(self.number(way, dist, part), here, self.place.ring(-way))
        if dist < 3 or (dist == 3 and part == (0 if way == 1 else 1)):
            self.board.send(self.number(way, dist + 1, part), here, here, self.place.ring(way))

    def items(self):
        out = []
        for dist in (1, 2, 3):
            for part in (0, 1):
                for way in (1, -1):
                    out.append((way, dist, part))
        out.append((1, 4, 0))
        out.append((-1, 4, 1))
        return out

    def drain(self):
        for part in (0, 1):
            for way in (1, -1):
                self.board.sent(self.number(way, 1, part), self.own[part], self.place.ring(way))
        for way, dist, part in self.items():
            if dist > 1:
                here = self.slot(way, dist - 1, part)
                self.board.sent(self.number(way, dist, part), here, self.place.ring(way))


def quarter_ref(buf, slot, part):
    if part == "U":
        return buf.at[slot]
    return buf.at[slot, part]


def attention_kernel(qt_ref, kvt_ref, ctx_ref, bias_ref, ow_ref, lat_ref, gate_ref, out_ref,
                     kvb, cbuf, owa, owb, s_a, s_b, mb_a, mb_b, m_ref, l_ref, acc, att, attb,
                     part_ref, sib_ref, sends, recvs):
    place = Place()
    board = Board(sends, recvs)
    kv_base = board.take(len(ITEM_ORDER))
    ctx_base = board.take(16)
    a2a_base = board.take(8)
    d2d = board.take(1)
    half_cols = D // 2
    ring = ZRing(board, place, (ow_ref.at[:, :half_cols], ow_ref.at[:, half_cols:]), (owa, owb))

    greet([place.sp_peer(k) for k in range(1, 16)] + [place.ring(k) for k in range(1, 8)]
          + [place.sibling()])

    def kv_send(key, src):
        axis, step, _ = ITEMS[key]
        h, da, db, part = key
        board.send(kv_base + ITEM_INDEX[key], src, quarter_ref(kvb, SLOT[key[:3]], part),
                   place.plane(axis, step))

    def own_part(h):
        return kvt_ref.at[h]

    for key in sorted((k for k in ITEMS if ITEMS[k][2] is None),
                      key=lambda k: 0 if ITEMS[k][0] == ("x" if k[0] == 0 else "y") else 1):
        kv_send(key, own_part(key[0]))
    ring.begin()
    for k in range(1, 16):
        board.send(ctx_base + k, ctx_ref, cbuf.at[place.s], place.sp_peer(k))
    cbuf[place.s] = ctx_ref[...]
    owa[place.z] = ow_ref[:, :half_cols]
    owb[place.z] = ow_ref[:, half_cols:]
    kvb[0] = kvt_ref[0]
    kvb[1] = kvt_ref[1]

    def kv_take(key):
        axis, step, _ = ITEMS[key]
        here = quarter_ref(kvb, SLOT[key[:3]], key[3])
        board.arrived(kv_base + ITEM_INDEX[key], here, place.plane(axis, -step))
        for other in ITEM_ORDER:
            if ITEMS[other][2] == key:
                src = here
                if key[3] == "U" and other[3] != "U":
                    src = kvb.at[SLOT[key[:3]], other[3]]
                kv_send(other, src)

    def ctx_unit():
        for k in range(1, 16):
            board.arrived(ctx_base + k, cbuf.at[(place.s - k + 16) % 16], place.sp_peer(16 - k))
        turned = cbuf[...].reshape(512, 256).astype(F32).T.astype(BF)
        for q in (0, 1):
            kvb[CTX_SLOT, q, 0:HEAD, :] = turned[0:HEAD, q * 256:(q + 1) * 256]
            kvb[CTX_SLOT, q, HEAD:HEAD + VDIM, :] = turned[128:128 + VDIM, q * 256:(q + 1) * 256]

    m_ref[...] = jnp.full(m_ref.shape, -jnp.inf, F32)
    l_ref[...] = jnp.zeros(l_ref.shape, F32)
    acc[...] = jnp.zeros(acc.shape, F32)

    def products(slot, s_ref, mb_ref):
        for q in (0, 1):
            keys = kvb[slot, q, 0:128, :].T
            for n in range(4):
                cols = slice(n * 256, (n + 1) * 256)
                scores = jnp.dot(keys, qt_ref[:, cols], preferred_element_type=F32)
                s_ref[q * 256:(q + 1) * 256, cols] = scores
                top = jnp.max(scores, axis=0, keepdims=True)
                mb_ref[:, cols] = top if q == 0 else jnp.maximum(mb_ref[:, cols], top)

    def absorb(slot, s_ref, mb_ref, bias):
        for n in range(4):
            cols = slice(n * 256, (n + 1) * 256)
            old = m_ref[:, cols]
            top = mb_ref[:, cols] * SCALE2
            if bias is not None:
                top = top + bias
            new = jnp.maximum(old, top)
            m_ref[:, cols] = new
            factor = jnp.exp2(old - new)
            less = new if bias is None else new - bias
            weights = jnp.exp2(s_ref[:, cols] * SCALE2 - less)
            l_ref[:, cols] = l_ref[:, cols] * factor + jnp.sum(weights, axis=0, keepdims=True)
            rounded = weights.astype(BF)
            summed = jnp.dot(kvb[slot, 0, HEAD:HEAD + VDIM, :], rounded[:256],
                             preferred_element_type=F32)
            summed = summed + jnp.dot(kvb[slot, 1, HEAD:HEAD + VDIM, :], rounded[256:],
                                      preferred_element_type=F32)
            acc[:, cols] = acc[:, cols] * factor + summed

    ring_items = ring.items()
    ring_plan = [[] for _ in range(N_UNITS)]
    for n, item in enumerate(ring_items):
        ring_plan[min(4 + (n * 26) // len(ring_items), N_UNITS - 1)].append(item)

    def actions(n):
        for key in PLAN[n]:
            kv_take(key)
        for item in ring_plan[n]:
            ring.take(*item)
        if n == CTX_SLOT:
            ctx_unit()

    def act_in_loop(i, offset):
        for trip in range(16):
            n = 2 * trip + offset
            if PLAN[n] or ring_plan[n] or n == CTX_SLOT:
                @pl.when(i == trip)
                def _():
                    actions(n)

    actions(0)
    products(0, s_a, mb_a)

    def body(i, carry):
        act_in_loop(i, 1)
        products(2 * i + 1, s_b, mb_b)
        absorb(2 * i, s_a, mb_a, None)
        act_in_loop(i, 2)
        products(2 * i + 2, s_a, mb_a)
        absorb(2 * i + 1, s_b, mb_b, None)
        return carry

    lax.fori_loop(0, 16, body, 0)
    bias = (bias_ref[0, 0] + math.log(TOK_DEV / CTX_DEV)) * LOG2E
    absorb(CTX_SLOT, s_a, mb_a, bias)

    for k in range(8):
        cols = slice(k * 128, (k + 1) * 128)
        att[k] = (acc[:, cols] / l_ref[:, cols]).astype(BF)
    for k in range(1, 8):
        board.send(a2a_base + k, att.at[(place.z + k) % 8], attb.at[place.z], place.ring(k))
    attb[place.z] = att[place.z]
    for k in range(1, 8):
        board.arrived(a2a_base + k, attb.at[(place.z - k + 8) % 8], place.ring(-k))
    rows = attb[...].reshape(8 * VDIM, 128).astype(F32).T.astype(BF)
    for n, weight in enumerate((owa, owb)):
        part_ref[:, n * half_cols:(n + 1) * half_cols] = jnp.dot(
            rows, weight[...].reshape(8 * VDIM, half_cols), preferred_element_type=F32)
    away = part_ref.at[pl.ds(pl.multiple_of(64 * (1 - place.c), 64), 64)]
    board.send(d2d, away, sib_ref, place.sibling())
    board.arrived(d2d, sib_ref, place.sibling())
    mine = part_ref[pl.ds(pl.multiple_of(64 * place.c, 64), 64)]
    projected = mine + sib_ref[...]
    out_ref[...] = (lat_ref[...].astype(F32) + gate_ref[...] * projected).astype(BF)

    board.sent(d2d, away, place.sibling())
    for k in range(1, 8):
        board.sent(a2a_base + k, att.at[(place.z + k) % 8], place.ring(k))
    for k in range(1, 16):
        board.sent(ctx_base + k, ctx_ref, place.sp_peer(k))
    ring.drain()
    for key in ITEM_ORDER:
        axis, step, _ = ITEMS[key]
        src = quarter_ref(kvb, 0, key[3])
        board.sent(kv_base + ITEM_INDEX[key], src, place.plane(axis, step))


def attention(qt, kvt, ctx, bias, out_weight, latent, gates):
    vmem = pl.BlockSpec(memory_space=pltpu.VMEM)
    copies = len(ITEM_ORDER) + 16 + 8 + 1 + 16
    return pl.pallas_call(
        attention_kernel,
        out_shape=jax.ShapeDtypeStruct((64, D), BF),
        in_specs=[vmem, vmem, vmem, pl.BlockSpec(memory_space=pltpu.SMEM), vmem, vmem, vmem],
        out_specs=vmem,
        scratch_shapes=[
            pltpu.VMEM((N_UNITS, 2, HEAD + VDIM, 256), BF),
            pltpu.VMEM((16, CTX_DEV, 256), BF),
            pltpu.VMEM((8, 64, D // 2), BF),
            pltpu.VMEM((8, 64, D // 2), BF),
            pltpu.VMEM((512, 1024), F32),
            pltpu.VMEM((512, 1024), F32),
            pltpu.VMEM((1, 1024), F32),
            pltpu.VMEM((1, 1024), F32),
            pltpu.VMEM((1, 1024), F32),
            pltpu.VMEM((1, 1024), F32),
            pltpu.VMEM((VDIM, 1024), F32),
            pltpu.VMEM((8, VDIM, 128), BF),
            pltpu.VMEM((8, VDIM, 128), BF),
            pltpu.VMEM((128, D), F32),
            pltpu.VMEM((64, D), F32),
            pltpu.SemaphoreType.DMA((copies,)),
            pltpu.SemaphoreType.DMA((copies,)),
        ],
        compiler_params=pltpu.CompilerParams(collective_id=0, has_side_effects=True,
                                             vmem_limit_bytes=50 * 1024 * 1024),
        cost_estimate=pl.CostEstimate(flops=6 * 10**9, bytes_accessed=10**7,
                                      transcendentals=17 * 10**6),
        name="attention",
    )(qt, kvt, ctx, bias, out_weight, latent, gates)


def sent_together(arrays, axis, dim, along):
    ends, at = ([], 0)
    for a in arrays[:-1]:
        at += a.shape[along]
        ends.append(at)
    both = jnp.concatenate(arrays, axis=along)
    return tuple(jnp.split(lax.all_gather(both, axis, axis=dim, tiled=True), ends, axis=along))


def rms_scale(tensor, gain):
    return (
        tensor
        * lax.rsqrt(jnp.mean(tensor * tensor, axis=-1, keepdims=True) + epsilon)
        * gain.astype(jnp.float32)
    )


def axial_tables(positions):
    pair_count = ROPE // 4
    frequency = jnp.power(theta, -jnp.arange(pair_count, dtype=jnp.float32) / pair_count)
    row_angle = (positions // GRID_W).astype(jnp.float32)[:, None] * frequency
    col_angle = (positions % GRID_W).astype(jnp.float32)[:, None] * frequency
    return (jnp.cos(row_angle), jnp.sin(row_angle), jnp.cos(col_angle), jnp.sin(col_angle))


def rotate_half(tensor, cosine, sine_table):
    first, second = jnp.split(tensor, 2, axis=-1)
    return jnp.concatenate(
        [first * cosine - second * sine_table, second * cosine + first * sine_table], axis=-1
    )


def axial_rotate(tensor, tables):
    half_width = tensor.shape[-1] // 2
    return jnp.concatenate(
        [
            rotate_half(tensor[..., :half_width], tables[0], tables[1]),
            rotate_half(tensor[..., half_width:], tables[2], tables[3]),
        ],
        axis=-1,
    )


def modulate(row_block, gain, shifts, scales):
    normal = rms_scale(row_block.astype(jnp.float32), gain)
    return (normal * (1.0 + scales) + shifts).astype(jnp.bfloat16)


def make_queries(query_latent, up_query, query_gain, tables):
    projected = jnp.dot(query_latent, up_query, preferred_element_type=jnp.float32)
    normal = rms_scale(projected, query_gain)
    return jnp.concatenate(
        [normal[..., :NOPE], axial_rotate(normal[..., NOPE:], tables)], axis=-1
    ).astype(jnp.bfloat16)


def make_keys(kv_latent, rope_rows, up_key, up_value, key_gain, tables):
    unrotated = jnp.dot(kv_latent, up_key, preferred_element_type=jnp.float32)
    normal = rms_scale(jnp.concatenate([unrotated, rope_rows.astype(F32)], axis=-1), key_gain)
    if tables is not None:
        normal = jnp.concatenate(
            [normal[..., :NOPE], axial_rotate(normal[..., NOPE:], tables)], axis=-1
        )
    values = jnp.dot(kv_latent, up_value, preferred_element_type=jnp.float32)
    return (normal.astype(jnp.bfloat16), values.astype(jnp.bfloat16))


def shards(
    latent,
    context,
    cond,
    cond_context,
    mod_weight,
    norm_gain,
    down_q,
    down_kv,
    rope_weight,
    qlat_gain,
    kvlat_gain,
    up_query,
    up_key,
    up_value,
    query_gain,
    key_gain,
    context_bias,
    out_weight,
):
    seq_index = lax.axis_index("sp")
    tp_count = lax.axis_size("tp")
    own_rows = latent.shape[0]
    block_tokens = own_rows * tp_count
    row_span = mod_weight.shape[1]
    activated = jax.nn.silu(jnp.stack([cond, cond_context]).astype(jnp.float32)).astype(
        jnp.bfloat16
    )
    own_part = lax.dynamic_slice_in_dim(activated, seq_index * row_span, row_span, 1)
    partial_value = jnp.concatenate(
        [
            jnp.einsum("d,rde->re", own_part[0], mod_weight, preferred_element_type=jnp.float32),
            jnp.einsum(
                "d,rde->re", own_part[1], mod_weight[:2], preferred_element_type=jnp.float32
            ),
        ],
        axis=0,
    )
    summed = lax.psum(partial_value, "sp")
    modulations = lax.all_gather(summed, "tp", axis=1, tiled=True)
    normed = modulate(latent, norm_gain, modulations[0], modulations[1])
    context_normed = modulate(context, norm_gain, modulations[3], modulations[4])
    stacked = jnp.concatenate([normed, context_normed], axis=0)
    pieces = sent_together((down_q, down_kv), "tp", 0, 1)
    query_down = jnp.dot(stacked[:own_rows], pieces[0], preferred_element_type=jnp.float32)
    kv_down = jnp.dot(stacked, pieces[1], preferred_element_type=jnp.float32)
    query_latent = rms_scale(query_down, qlat_gain).astype(jnp.bfloat16)
    kv_latent = rms_scale(kv_down, kvlat_gain).astype(jnp.bfloat16)
    rope_rows = jnp.dot(stacked, rope_weight, preferred_element_type=jnp.float32).astype(
        jnp.bfloat16
    )
    all_query, all_kv, all_rope = sent_together(
        (query_latent, kv_latent[:own_rows], rope_rows[:own_rows]), "tp", 0, 1
    )
    ck, cv = make_keys(
        kv_latent[own_rows:], rope_rows[own_rows:], up_key, up_value, key_gain, None
    )
    positions = seq_index * block_tokens + jnp.arange(block_tokens, dtype=jnp.int32)
    tables = axial_tables(positions)
    queries = make_queries(all_query, up_query, query_gain, tables)
    keys, values = make_keys(all_kv, all_rope, up_key, up_value, key_gain, tables)
    qt = jnp.pad(queries, ((0, 0), (0, 128 - HEAD))).T
    kvt = jnp.concatenate([keys, values], axis=1).T
    kvt = kvt.reshape(HEAD + VDIM, 2, 2, 256).transpose(1, 2, 0, 3)
    ctx = jnp.concatenate(
        [jnp.pad(ck, ((0, 0), (0, 128 - HEAD))), jnp.pad(cv, ((0, 0), (0, 128 - VDIM)))], axis=1
    )
    gates = modulations[2:3]
    return attention(qt, kvt, ctx, context_bias.reshape(1, 1), out_weight, latent, gates)


def solution(mesh):
    placed = (
        P(SP_TP, None),
        P("sp", None),
        P(),
        P(),
        P(None, "sp", "tp"),
        P(),
        P("tp", None),
        P("tp", None),
        P(),
        P(),
        P(),
        P(None, "tp"),
        P(None, "tp"),
        P(None, "tp"),
        P(),
        P(),
        P("tp"),
        P("tp", None),
    )
    return jax.shard_map(
        shards, mesh=mesh, in_specs=placed, out_specs=P(SP_TP, None), check_vma=False
    )
```

time: 258 us -> 190 us (0.74)
  Pallas kernels: 0 us -> 54 us
  matrix products: 59.1 us -> 12.1 us
  waiting for transfers between devices: 71.7 us -> 32.3 us
  blocking collectives: 79 us -> 62.1 us
  other arithmetic: 23.2 us -> 10.8 us
  local copies, waits for them, and re-layouts: 9.15 us -> 3.71 us
    pallas_call x0 -> x1, Pallas kernels: none -> 54 us  [attention(): pl.pallas_call(attention_kernel, out_shape=jax.ShapeDtypeStruct((64, D),...]
    dot_general x41 -> x6, matrix products: 54 us -> 8.37 us  [the longest x1 2.63 us: shards(): jnp.dot(stacked[:own_rows], pieces[0], preferred_element_type=jnp.float32)]
    all_gather x3 -> x2, waiting for transfers between devices: 71.1 us -> 32.2 us  [sent_together(): lax.all_gather(both, axis, axis=dim, tiled=True)]
    all_gather x1 -> x0, blocking collectives: 19.7 us -> none  [sent_together(): lax.all_gather(both, axis, axis=dim, tiled=True)]
    all_to_all x1 -> x0, blocking collectives: 16.6 us -> none  [shards(): lax.all_to_all(attended, 'tp', split_axis=0, concat_axis=1, tiled=True)]
    psum x2 -> x1, blocking collectives: 18.4 us -> 34.2 us  [shards(): summed = lax.psum(partial_value, 'sp')]
    reduce_sum x17 -> x0, other arithmetic: 12.1 us -> none  [absorb_block(): run_sum = run_sum * factor + jnp.sum(weights, axis=-1)]
    all_gather x1, blocking collectives: 24.3 us -> 27.9 us  [shards(): modulations = lax.all_gather(summed, 'tp', axis=1, tiled=True)]
  transfers between devices with their start and end apart: 4 -> 2, of which waited for: 2 -> 1; matrix products, arithmetic and copies ran while one was open for 26% -> 6% of each run, Pallas kernels for 0% -> 0%
where the time goes in v1:
time: 190 us; the launch traced here: 189 us
  blocking collectives  62.1 us (33%)
  Pallas kernels  54 us (28%)
  waiting for transfers between devices  32.3 us (17%)
  between operations  14.4 us (8%)
  matrix products  12.1 us (6%)
  other arithmetic  10.8 us (6%)
  local copies, waits for them, and re-layouts  3.71 us (2%)
    pallas_call x1, Pallas kernels, attention(): pl.pallas_call(attention_kernel, out_shape=jax.ShapeDtypeStruct((64, D),...  54 us
    psum x1, blocking collectives, shards(): summed = lax.psum(partial_value, 'sp')  34.2 us
    all_gather x2, waiting for transfers between devices, sent_together(): lax.all_gather(both, axis, axis=dim, tiled=True)  32.2 us
    all_gather x1, blocking collectives, shards(): modulations = lax.all_gather(summed, 'tp', axis=1, tiled=True)  27.9 us
  transfers between devices with their start and end apart: 2, of which 1 were waited for; matrix products, arithmetic and copies ran while one was open for 6% of the time, Pallas kernels for 0%

profile of v1, /device:TPU:1, one launch (start us, length us, event | category | flops | bytes accessed | tf_op | source)
XLA Modules:
  0.0 189.4 jit_solution(8896431744563661467)
XLA Ops:
  6.5 1.8 pad_maximum_fusion.2
  8.4 0.7 stack.10
  9.1 0.7 stack.9
  9.8 1.0 fusion.71
  10.9 0.7 convert_element_type.75
  11.6 0.7 convert_element_type.83
  12.2 0.7 convert_element_type.79
  12.9 1.0 fusion.22
  13.9 34.2 %psum.7 = f32[5,128]{1,0:T(8,128)S(1)} all-reduce(f32[5,128]{1,0:T(8,128)S(1)} %pad_maximum_fusion.7), channel_id=1, replica_groups=mesh['sp'=16,'tp'=16] {'sp'}, use_global_device_ids=true, to_apply=%region_1.2 | all-reduce | flops 640 | bytes 5120 | tf_op jit(solution)/shard_map/psum | solution.py:528
  48.1 27.9 %all_gather.9 = f32[5,2048]{1,0:T(8,128)S(1)} all-gather(f32[5,128]{1,0:T(8,128)S(1)} %psum.7), channel_id=1, replica_groups=mesh['sp'=16,'tp'=16] {'tp'}, dimensions={1}, use_global_device_ids=true | all-gather | bytes 43520 | tf_op jit(solution)/shard_map/all_gather | solution.py:529
  76.0 1.0 fusion.15
  77.0 1.1 fusion.10
  78.2 1.0 fusion.19
  79.3 1.1 fusion.14
  80.4 1.2 convolution_convert_fusion.1
  81.6 2.2 %multiply_reduce_fusion.2 = (f32[96]{0:T(128)S(1)}, f32[96,512]{1,0:T(8,128)S(1)}) fusion(bf16[2048,1280]{1,0:T(8,128)(2,1)} %all-gather.3.cloned.1.call-done, bf16[32,2048]{1,0:T(8,128)(2,1)S(1)} %fusion.19, bf16[64,2048]{1,0:T(8,128)(2,1)S(1)} %fusion.14), kind=kOutput, calls=%fused_computation.39 | convolution fusion | flops 202211232 | bytes 2687360 | tf_op jit(solution)/shard_map/dot_general | solution.py:535
  83.9 2.6 %multiply_reduce_fusion.3 = (f32[64]{0:T(128)S(1)}, f32[64,768]{1,0:T(8,128)S(1)}) fusion(bf16[64,2048]{1,0:T(8,128)(2,1)S(1)} %fusion.14, bf16[2048,1280]{1,0:T(8,128)(2,1)} %all-gather.3.cloned.1.call-done), kind=kOutput, calls=%fused_computation.41 | convolution fusion | flops 201424832 | bytes 3604736 | tf_op jit(solution)/shard_map/dot_general | solution.py:534
  86.7 0.7 pad_maximum_fusion.5
  88.2 0.2 multiply_reduce_fusion.4
  88.7 32.2 %all-gather.5.cloned.1.call-done = bf16[1024,1312]{1,0:T(8,128)(2,1)} async-done(((bf16[64,1312]{1,0:T(8,128)(2,1)}), bf16[1024,1312]{1,0:T(8,128)(2,1)}) %all-gather.5.cloned.1.call-update) | async-done | bytes 2686992 | tf_op jit(solution)/shard_map/all_gather | solution.py:429
  120.9 1.1 split.60
  122.2 1.7 fusion.8
  123.9 0.6 multiply_reduce_fusion.1
  124.8 0.2 constant_dynamic-update-slice_fusion.7
  125.0 0.2 constant_dynamic-update-slice_fusion.6
  125.2 0.3 constant_dynamic-update-slice_fusion.5
  125.5 0.2 constant_dynamic-update-slice_fusion.4
  125.7 1.7 fusion.6
  127.4 0.2 reshape.107
  127.7 0.2 constant_dynamic-update-slice_fusion
  127.9 54.0 %attention.1 = bf16[64,2048]{1,0:T(8,128)(2,1)S(1)} custom-call(bf16[128,1024]{1,0:T(8,128)(2,1)S(1)} %pad_bitcast_fusion.qt_ref, bf16[2,2,160,256]{3,2,1,0:T(8,128)(2,1)S(1)} %bitcast.37, bf16[32,256]{1,0:T(8,128)(2,1)S(1)} %fusion.61.ctx_ref, f32[1,1]{1,0:T(1,128)} %bitcast.36.bias_ref, bf16[64,2048]{1,0:T(8,128)(2,1)S(1)} %copy-done.2, ...), custom_call_target="tpu_custom_call" | custom-call | flops 6000000000 | bytes 10000000 | tf_op jit(solution)/shard_map/attention/pallas_call | solution.py:391
  181.9 0.7 copy.50
  (53 shorter events, 1.3 us)
Async XLA Ops:
  6.5 117.4 %copy-start = (bf16[768,96]{0,1:T(8,128)(2,1)S(1)}, bf16[768,96]{0,1:T(8,128)(2,1)}, u32[]{:S(2)}) copy-start(bf16[768,96]{0,1:T(8,128)(2,1)} %param.29) | copy-start | bytes 442372
  6.5 75.0 %all-gather.3.cloned.1.call-start = ((), (), s32[]{:S(2)}) async-start(), calls=%async_computation | async-start | bytes 5570560 | tf_op jit(solution)/shard_map/all_gather | solution.py:429
  8.3 112.6 %all-gather.5.cloned.1.call-start = ((), (), s32[]{:S(2)}) async-start(), calls=%async_computation.1 | async-start | bytes 3063808 | tf_op jit(solution)/shard_map/all_gather | solution.py:429
  83.8 4.3 %copy-start.3 = (bf16[512,64]{0,1:T(8,128)(2,1)S(1)}, bf16[512,64]{0,1:T(8,128)(2,1)}, u32[]{:S(2)}) copy-start(bf16[512,64]{0,1:T(8,128)(2,1)} %param.30) | copy-start | bytes 196612
  83.8 4.7 %copy-start.6 = (f32[96]{0:T(128)S(1)}, f32[96]{0:T(128)}, u32[]{:S(2)}) copy-start(f32[96]{0:T(128)} %param.33) | copy-start | bytes 1156
  83.8 4.7 %copy-start.4 = (bf16[512,64]{0,1:T(8,128)(2,1)S(1)}, bf16[512,64]{0,1:T(8,128)(2,1)}, u32[]{:S(2)}) copy-start(bf16[512,64]{0,1:T(8,128)(2,1)} %param.31) | copy-start | bytes 196612
  88.2 36.3 %copy-start.7 = (f32[96]{0:T(128)S(1)}, f32[96]{0:T(128)}, u32[]{:S(2)}) copy-start(f32[96]{0:T(128)} %param.32) | copy-start | bytes 1156
  120.9 3.0 %copy-start.5 = (bf16[1024,1312]{1,0:T(8,128)(2,1)S(1)}, bf16[1024,1312]{1,0:T(8,128)(2,1)}, u32[]{:S(2)}) copy-start(bf16[1024,1312]{1,0:T(8,128)(2,1)} %all-gather.5.cloned.1.call-done) | copy-start | bytes 8060932
  124.6 3.3 %copy-start.1 = (bf16[64,2048]{1,0:T(8,128)(2,1)S(1)}, bf16[64,2048]{1,0:T(8,128)(2,1)}, u32[]{:S(2)}) copy-start(bf16[64,2048]{1,0:T(8,128)(2,1)} %lat_ref.1) | copy-start | bytes 786436
  124.6 3.3 %copy-start.2 = (bf16[64,2048]{1,0:T(8,128)(2,1)S(1)}, bf16[64,2048]{1,0:T(8,128)(2,1)}, u32[]{:S(2)}) copy-start(bf16[64,2048]{1,0:T(8,128)(2,1)} %ow_ref.1) | copy-start | bytes 786436
Sparse Core Ops, SparseCore 0:
  9.2 47.3 all-gather.2
  87.5 33.3 all-gather.4

commit v2 on v1

--- a/solution.py
+++ b/solution.py
@@ -1,8 +1,8 @@
-import functools
 import math
 
 import jax
 import jax.numpy as jnp
+import numpy as np
 from jax import lax
 from jax.experimental import pallas as pl
 from jax.experimental.pallas import tpu as pltpu
@@ -180,21 +180,26 @@
 
 
 class ZRing:
-    def __init__(self, board, place, own, bufs):
+    def __init__(self, board, place, own, bufs, by_device=False):
         self.board, self.place, self.own, self.bufs = board, place, own, bufs
+        self.by_device = by_device
         self.base = board.take(16)
 
     def number(self, way, dist, part):
         return self.base + (0 if way == 1 else 8) + (dist - 1) * 2 + part
 
     def slot(self, way, dist, part):
-        return self.bufs[part].at[(self.place.z - way * dist + 16) % 8]
+        return self.bufs[part].at[self.index(way * dist)]
+
+    def index(self, back):
+        at = (self.place.z - back + 16) % 8
+        return at * 2 + self.place.c if self.by_device else at
 
     def begin(self):
         for part in (0, 1):
             for way in (1, -1):
                 self.board.send(self.number(way, 1, part), self.own[part],
-                                self.bufs[part].at[self.place.z], self.place.ring(way))
+                                self.bufs[part].at[self.index(0)], self.place.ring(way))
 
     def take(self, way, dist, part):
         here = self.slot(way, dist, part)
@@ -228,20 +233,208 @@
     return buf.at[slot, part]
 
 
-def attention_kernel(qt_ref, kvt_ref, ctx_ref, bias_ref, ow_ref, lat_ref, gate_ref, out_ref,
-                     kvb, cbuf, owa, owb, s_a, s_b, mb_a, mb_b, m_ref, l_ref, acc, att, attb,
-                     part_ref, sib_ref, sends, recvs):
+def whole_kernel(lat_ref, context_ref, cond_ref, condc_ref, mw_ref, ng_ref, dq_ref, dkv_ref,
+                 rw_ref, qlg_ref, kvlg_ref, upq_ref, upk_ref, upv_ref, qg_ref, kg_ref, bias_ref,
+                 ow_ref, base_ref, tab_ref, out_ref,
+                 wq, wkv, latsib, modp, modf, xn, uq, ukv, sq, skv, lq, lk, upt, wk, pad,
+                 qt, kvb, cbuf, owa, owb, s_a, s_b, mb_a, mb_b, m_ref, l_ref, acc, att, attb,
+                 part_ref, sib_ref, sends, recvs):
     place = Place()
     board = Board(sends, recvs)
     kv_base = board.take(len(ITEM_ORDER))
     ctx_base = board.take(16)
     a2a_base = board.take(8)
     d2d = board.take(1)
+    lat_d2d = board.take(1)
+    modp_base = board.take(16)
+    modf_base = board.take(16)
+    part_base = board.take(2)
+    share_base = board.take(16)
     half_cols = D // 2
     ring = ZRing(board, place, (ow_ref.at[:, :half_cols], ow_ref.at[:, half_cols:]), (owa, owb))
-
-    greet([place.sp_peer(k) for k in range(1, 16)] + [place.ring(k) for k in range(1, 8)]
-          + [place.sibling()])
+    wring = ZRing(board, place, (dq_ref, dkv_ref), (wq, wkv))
+    lring = ZRing(board, place, (lq.at[place.t], lk.at[place.t]), (lq, lk), by_device=True)
+
+    greet([place.sp_peer(k) for k in range(1, 16)] + [place.tp_peer(k) for k in range(1, 16)])
+
+    wring.begin()
+    board.send(lat_d2d, lat_ref, latsib, place.sibling())
+
+    span = pl.ds(pl.multiple_of(place.s * 128, 128), 128)
+
+    def silu(v):
+        v = v.astype(F32)
+        return v / (1.0 + jnp.exp(-v))
+
+    act = jnp.concatenate(
+        [silu(cond_ref[:, span]), silu(condc_ref[:, span]), jnp.zeros((14, 128), F32)],
+        axis=0).astype(BF)
+    terms = [jnp.dot(act, mw_ref[r], preferred_element_type=F32) for r in range(3)]
+    modp[place.s] = jnp.concatenate(
+        [terms[0][0:1], terms[1][0:1], terms[2][0:1], terms[0][1:2], terms[1][1:2],
+         jnp.zeros((3, 128), F32)], axis=0)
+    for k in range(1, 16):
+        board.send(modp_base + k, modp.at[place.s], modp.at[place.s], place.sp_peer(k))
+
+    wq[place.z] = dq_ref[...]
+    wkv[place.z] = dkv_ref[...]
+    owa[place.z] = ow_ref[:, :half_cols]
+    owb[place.z] = ow_ref[:, half_cols:]
+    pad[...] = jnp.zeros(pad.shape, F32)
+    pad[:, 0:HEAD] = upq_ref[...].astype(F32)
+    upt[...] = pad[...].T.astype(BF)
+    wk[...] = jnp.zeros(wk.shape, BF)
+    pad[0:512, 0:NOPE] = upk_ref[...].astype(F32)
+    pad[0:512, NOPE:128] = upv_ref[...].astype(F32)
+    turned_up = pad[0:512, :].T.astype(BF)
+    wk[0:NOPE, 0:512] = turned_up[0:NOPE]
+    wk[HEAD:HEAD + VDIM, 0:512] = turned_up[NOPE:128]
+    unit = (lax.broadcasted_iota(jnp.int32, (ROPE, 128), 0)
+            == lax.broadcasted_iota(jnp.int32, (ROPE, 128), 1))
+    wk[NOPE:HEAD, 512:640] = jnp.where(unit, 1.0, 0.0).astype(BF)
+
+    def inverse(ref):
+        rows = ref[...].astype(F32)
+        return lax.rsqrt(jnp.mean(rows * rows, axis=-1, keepdims=True) + epsilon)
+
+    inv_own = inverse(lat_ref)
+    inv_ctx = inverse(context_ref)
+
+    for k in range(1, 16):
+        board.arrived(modp_base + k, modp.at[(place.s - k + 16) % 16], place.sp_peer(16 - k))
+    modf[place.t] = jnp.sum(modp[...], axis=0)
+    for k in range(1, 16):
+        board.send(modf_base + k, modf.at[place.t], modf.at[place.t], place.tp_peer(k))
+
+    board.arrived(lat_d2d, latsib, place.sibling())
+    inv_sib = inverse(latsib)
+    w_items = wring.items()
+    for item in w_items[:4]:
+        wring.take(*item)
+    for k in range(1, 16):
+        board.arrived(modf_base + k, modf.at[(place.t - k + 16) % 16], place.tp_peer(16 - k))
+
+    for k in range(16):
+        cols = slice(k * 128, (k + 1) * 128)
+        gain = ng_ref[:, cols].astype(F32)
+        shift, scale = modf[k, 0:1, :], modf[k, 1:2, :]
+        own = lat_ref[:, cols].astype(F32) * inv_own * gain
+        xn[k, 0:64] = (own * (1.0 + scale) + shift).astype(BF)
+        sib = latsib[:, cols].astype(F32) * inv_sib * gain
+        xn[k, 96:160] = (sib * (1.0 + scale) + shift).astype(BF)
+        ctx = context_ref[:, cols].astype(F32) * inv_ctx * gain
+        xn[k, 64:96] = (ctx * (1.0 + modf[k, 4:5, :]) + modf[k, 3:4, :]).astype(BF)
+
+    def add_product(at, part):
+        rows = xn[2 * at + place.c]
+        if part == 0:
+            uq[...] += jnp.dot(rows, wq[at], preferred_element_type=F32)
+        else:
+            ukv[...] += jnp.dot(rows, wkv[at], preferred_element_type=F32)
+
+    uq[...] = jnp.dot(xn[place.t], wq[place.z], preferred_element_type=F32)
+    ukv[...] = jnp.dot(xn[place.t], wkv[place.z], preferred_element_type=F32)
+    rope = jnp.dot(xn[0, 0:96], rw_ref[0:128], preferred_element_type=F32)
+    for k in range(1, 16):
+        rope = rope + jnp.dot(xn[k, 0:96], rw_ref[k * 128:(k + 1) * 128],
+                              preferred_element_type=F32)
+    rope = rope.astype(BF).astype(F32)
+    for n, (way, dist, part) in enumerate(w_items):
+        if n >= 4:
+            wring.take(way, dist, part)
+        add_product(wring.index(way * dist), part)
+
+    board.send(part_base, uq.at[96:160], sq, place.sibling())
+    board.send(part_base + 1, ukv.at[64:160], skv, place.sibling())
+
+    def latent_of(total, gain_ref):
+        return (total * lax.rsqrt(jnp.mean(total * total, axis=-1, keepdims=True) + epsilon)
+                * gain_ref[...].astype(F32)).astype(BF)
+
+    board.arrived(part_base, sq, place.sibling())
+    lq[place.t] = latent_of(uq[0:64] + sq[...], qlg_ref)
+    board.arrived(part_base + 1, skv, place.sibling())
+    lk[place.t, :, 0:512] = latent_of(ukv[0:64] + skv[32:96], kvlg_ref)
+    lk[place.t, :, 512:640] = jnp.concatenate(
+        [rope[0:64], jnp.zeros((64, 96), F32)], axis=1).astype(BF)
+    lring.begin()
+
+    def share(number, ref):
+        board.send(share_base + number, ref, ref, place.sibling())
+
+    share(0, lq.at[place.t])
+    share(1, lk.at[place.t])
+
+    ctx_kv = latent_of(ukv[64:96] + skv[0:32], kvlg_ref)
+    ctx_k = jnp.dot(ctx_kv, upk_ref[...], preferred_element_type=F32)
+    ctx_v = jnp.dot(ctx_kv, upv_ref[...], preferred_element_type=F32)
+    ctx_u = jnp.concatenate([ctx_k, rope[64:96]], axis=1)
+    ctx_n = ctx_u * lax.rsqrt(jnp.mean(ctx_u * ctx_u, axis=-1, keepdims=True) + epsilon)
+    ctx_n = ctx_n * kg_ref[...]
+    cbuf[place.s] = jnp.concatenate(
+        [ctx_n, jnp.zeros((CTX_DEV, 128 - HEAD), F32), ctx_v,
+         jnp.zeros((CTX_DEV, 128 - VDIM), F32)], axis=1).astype(BF)
+    for k in range(1, 16):
+        board.send(ctx_base + k, cbuf.at[place.s], cbuf.at[place.s], place.sp_peer(k))
+
+    base = base_ref[pl.ds(pl.multiple_of(place.s * 16, 16), 16)]
+    base_cos, base_sin = base[0:8, 0:1], base[8:16, 0:1]
+    row_cos = tab_ref[0:8] * base_cos - tab_ref[8:16] * base_sin
+    row_sin = tab_ref[8:16] * base_cos + tab_ref[0:8] * base_sin
+    col_cos, col_sin = tab_ref[16:24], tab_ref[24:32]
+
+    def column(gain_ref):
+        row = jnp.concatenate([gain_ref[...], jnp.zeros((1, 128 - HEAD), F32)], axis=1)
+        return jnp.broadcast_to(row, (128, 128)).T[0:HEAD, 0:1]
+
+    def turned(u, gain):
+        normal = u * lax.rsqrt(jnp.mean(u * u, axis=0, keepdims=True) + epsilon) * gain
+        a, b, c, d = (normal[NOPE + 8 * n:NOPE + 8 * n + 8] for n in range(4))
+        return jnp.concatenate(
+            [normal[0:NOPE], a * row_cos - b * row_sin, b * row_cos + a * row_sin,
+             c * col_cos - d * col_sin, d * col_cos + c * col_sin], axis=0)
+
+    query_gain, key_gain = column(qg_ref), column(kg_ref)
+
+    own_at = [(1, 0), (-1, 0)]
+    for n, (way, dist, part) in enumerate(lring.items()):
+        lring.take(way, dist, part)
+        share(2 + n, lring.slot(way, dist, part))
+    other = 1 - place.c
+    for part, buf in enumerate((lq, lk)):
+        board.arrived(share_base + part, buf.at[place.z * 2 + other], place.sibling())
+    for n, (way, dist, part) in enumerate(lring.items()):
+        at = ((place.z - way * dist + 16) % 8) * 2 + other
+        board.arrived(share_base + 2 + n, (lq, lk)[part].at[at], place.sibling())
+
+    contract = (((1,), (1,)), ((), ()))
+    kv = lax.dot_general(wk[...], lk[...].reshape(1024, 640), contract,
+                         preferred_element_type=F32)
+    kv = jnp.concatenate([turned(kv[0:HEAD], key_gain), kv[HEAD:HEAD + VDIM]],
+                         axis=0).astype(BF)
+    for h in (0, 1):
+        for q in (0, 1):
+            at = (2 * h + q) * 256
+            kvb[SLOT[(h, 0, 0)], q] = kv[:, at:at + 256]
+
+    def queries():
+        u = lax.dot_general(upt[...], lq[...].reshape(1024, 768), contract,
+                            preferred_element_type=F32)
+        qt[0:HEAD] = turned(u[0:HEAD], query_gain).astype(BF)
+        qt[HEAD:128] = jnp.zeros((128 - HEAD, 1024), BF)
+
+    def finish():
+        wring.drain()
+        lring.drain()
+        board.sent(lat_d2d, lat_ref, place.sibling())
+        for k in range(1, 16):
+            board.sent(modp_base + k, modp.at[place.s], place.sp_peer(k))
+            board.sent(modf_base + k, modf.at[place.t], place.tp_peer(k))
+        board.sent(part_base, uq.at[96:160], place.sibling())
+        board.sent(part_base + 1, ukv.at[64:160], place.sibling())
+        share_sizes = [0, 1] + [item[2] for item in lring.items()]
+        for n, part in enumerate(share_sizes):
+            board.sent(share_base + n, (lq, lk)[part].at[0], place.sibling())
 
     def kv_send(key, src):
         axis, step, _ = ITEMS[key]
@@ -250,19 +443,13 @@
                    place.plane(axis, step))
 
     def own_part(h):
-        return kvt_ref.at[h]
+        return kvb.at[SLOT[(h, 0, 0)]]
 
     for key in sorted((k for k in ITEMS if ITEMS[k][2] is None),
                       key=lambda k: 0 if ITEMS[k][0] == ("x" if k[0] == 0 else "y") else 1):
         kv_send(key, own_part(key[0]))
     ring.begin()
-    for k in range(1, 16):
-        board.send(ctx_base + k, ctx_ref, cbuf.at[place.s], place.sp_peer(k))
-    cbuf[place.s] = ctx_ref[...]
-    owa[place.z] = ow_ref[:, :half_cols]
-    owb[place.z] = ow_ref[:, half_cols:]
-    kvb[0] = kvt_ref[0]
-    kvb[1] = kvt_ref[1]
+    queries()
 
     def kv_take(key):
         axis, step, _ = ITEMS[key]
@@ -292,7 +479,7 @@
             keys = kvb[slot, q, 0:128, :].T
             for n in range(4):
                 cols = slice(n * 256, (n + 1) * 256)
-                scores = jnp.dot(keys, qt_ref[:, cols], preferred_element_type=F32)
+                scores = jnp.dot(keys, qt[:, cols], preferred_element_type=F32)
                 s_ref[q * 256:(q + 1) * 256, cols] = scores
                 top = jnp.max(scores, axis=0, keepdims=True)
                 mb_ref[:, cols] = top if q == 0 else jnp.maximum(mb_ref[:, cols], top)
@@ -369,122 +556,34 @@
     away = part_ref.at[pl.ds(pl.multiple_of(64 * (1 - place.c), 64), 64)]
     board.send(d2d, away, sib_ref, place.sibling())
     board.arrived(d2d, sib_ref, place.sibling())
+    gates = jnp.concatenate([modf[k, 2:3, :] for k in range(16)], axis=1)
     mine = part_ref[pl.ds(pl.multiple_of(64 * place.c, 64), 64)]
     projected = mine + sib_ref[...]
-    out_ref[...] = (lat_ref[...].astype(F32) + gate_ref[...] * projected).astype(BF)
+    out_ref[...] = (lat_ref[...].astype(F32) + gates * projected).astype(BF)
 
     board.sent(d2d, away, place.sibling())
     for k in range(1, 8):
         board.sent(a2a_base + k, att.at[(place.z + k) % 8], place.ring(k))
     for k in range(1, 16):
-        board.sent(ctx_base + k, ctx_ref, place.sp_peer(k))
+        board.sent(ctx_base + k, cbuf.at[place.s], place.sp_peer(k))
     ring.drain()
+    finish()
     for key in ITEM_ORDER:
         axis, step, _ = ITEMS[key]
         src = quarter_ref(kvb, 0, key[3])
         board.sent(kv_base + ITEM_INDEX[key], src, place.plane(axis, step))
 
 
-def attention(qt, kvt, ctx, bias, out_weight, latent, gates):
-    vmem = pl.BlockSpec(memory_space=pltpu.VMEM)
-    copies = len(ITEM_ORDER) + 16 + 8 + 1 + 16
-    return pl.pallas_call(
-        attention_kernel,
-        out_shape=jax.ShapeDtypeStruct((64, D), BF),
-        in_specs=[vmem, vmem, vmem, pl.BlockSpec(memory_space=pltpu.SMEM), vmem, vmem, vmem],
-        out_specs=vmem,
-        scratch_shapes=[
-            pltpu.VMEM((N_UNITS, 2, HEAD + VDIM, 256), BF),
-            pltpu.VMEM((16, CTX_DEV, 256), BF),
-            pltpu.VMEM((8, 64, D // 2), BF),
-            pltpu.VMEM((8, 64, D // 2), BF),
-            pltpu.VMEM((512, 1024), F32),
-            pltpu.VMEM((512, 1024), F32),
-            pltpu.VMEM((1, 1024), F32),
-            pltpu.VMEM((1, 1024), F32),
-            pltpu.VMEM((1, 1024), F32),
-            pltpu.VMEM((1, 1024), F32),
-            pltpu.VMEM((VDIM, 1024), F32),
-            pltpu.VMEM((8, VDIM, 128), BF),
-            pltpu.VMEM((8, VDIM, 128), BF),
-            pltpu.VMEM((128, D), F32),
-            pltpu.VMEM((64, D), F32),
-            pltpu.SemaphoreType.DMA((copies,)),
-            pltpu.SemaphoreType.DMA((copies,)),
-        ],
-        compiler_params=pltpu.CompilerParams(collective_id=0, has_side_effects=True,
-                                             vmem_limit_bytes=50 * 1024 * 1024),
-        cost_estimate=pl.CostEstimate(flops=6 * 10**9, bytes_accessed=10**7,
-                                      transcendentals=17 * 10**6),
-        name="attention",
-    )(qt, kvt, ctx, bias, out_weight, latent, gates)
-
-
-def sent_together(arrays, axis, dim, along):
-    ends, at = ([], 0)
-    for a in arrays[:-1]:
-        at += a.shape[along]
-        ends.append(at)
-    both = jnp.concatenate(arrays, axis=along)
-    return tuple(jnp.split(lax.all_gather(both, axis, axis=dim, tiled=True), ends, axis=along))
-
-
-def rms_scale(tensor, gain):
-    return (
-        tensor
-        * lax.rsqrt(jnp.mean(tensor * tensor, axis=-1, keepdims=True) + epsilon)
-        * gain.astype(jnp.float32)
-    )
-
-
-def axial_tables(positions):
-    pair_count = ROPE // 4
-    frequency = jnp.power(theta, -jnp.arange(pair_count, dtype=jnp.float32) / pair_count)
-    row_angle = (positions // GRID_W).astype(jnp.float32)[:, None] * frequency
-    col_angle = (positions % GRID_W).astype(jnp.float32)[:, None] * frequency
-    return (jnp.cos(row_angle), jnp.sin(row_angle), jnp.cos(col_angle), jnp.sin(col_angle))
-
-
-def rotate_half(tensor, cosine, sine_table):
-    first, second = jnp.split(tensor, 2, axis=-1)
-    return jnp.concatenate(
-        [first * cosine - second * sine_table, second * cosine + first * sine_table], axis=-1
-    )
-
-
-def axial_rotate(tensor, tables):
-    half_width = tensor.shape[-1] // 2
-    return jnp.concatenate(
-        [
-            rotate_half(tensor[..., :half_width], tables[0], tables[1]),
-            rotate_half(tensor[..., half_width:], tables[2], tables[3]),
-        ],
-        axis=-1,
-    )
-
-
-def modulate(row_block, gain, shifts, scales):
-    normal = rms_scale(row_block.astype(jnp.float32), gain)
-    return (normal * (1.0 + scales) + shifts).astype(jnp.bfloat16)
-
-
-def make_queries(query_latent, up_query, query_gain, tables):
-    projected = jnp.dot(query_latent, up_query, preferred_element_type=jnp.float32)
-    normal = rms_scale(projected, query_gain)
-    return jnp.concatenate(
-        [normal[..., :NOPE], axial_rotate(normal[..., NOPE:], tables)], axis=-1
-    ).astype(jnp.bfloat16)
-
-
-def make_keys(kv_latent, rope_rows, up_key, up_value, key_gain, tables):
-    unrotated = jnp.dot(kv_latent, up_key, preferred_element_type=jnp.float32)
-    normal = rms_scale(jnp.concatenate([unrotated, rope_rows.astype(F32)], axis=-1), key_gain)
-    if tables is not None:
-        normal = jnp.concatenate(
-            [normal[..., :NOPE], axial_rotate(normal[..., NOPE:], tables)], axis=-1
-        )
-    values = jnp.dot(kv_latent, up_value, preferred_element_type=jnp.float32)
-    return (normal.astype(jnp.bfloat16), values.astype(jnp.bfloat16))
+def rotation_tables():
+    frequency = np.power(np.float32(theta), -np.arange(8, dtype=np.float32) / np.float32(8))
+    frequency = frequency.astype(np.float32).astype(np.float64)[:, None]
+    token = np.arange(1024)[None, :]
+    row, col = frequency * (token // GRID_W), frequency * (token % GRID_W)
+    table = np.concatenate([np.cos(row), np.sin(row), np.cos(col), np.sin(col)])
+    first = frequency * (np.arange(16)[None, :] * 16)
+    base = np.stack([np.cos(first), np.sin(first)]).reshape(16, 16).T.reshape(256, 1)
+    base = np.broadcast_to(base, (256, 128))
+    return base.astype(np.float32), table.astype(np.float32)
 
 
 def shards(
@@ -507,55 +606,58 @@
     context_bias,
     out_weight,
 ):
-    seq_index = lax.axis_index("sp")
-    tp_count = lax.axis_size("tp")
-    own_rows = latent.shape[0]
-    block_tokens = own_rows * tp_count
-    row_span = mod_weight.shape[1]
-    activated = jax.nn.silu(jnp.stack([cond, cond_context]).astype(jnp.float32)).astype(
-        jnp.bfloat16
-    )
-    own_part = lax.dynamic_slice_in_dim(activated, seq_index * row_span, row_span, 1)
-    partial_value = jnp.concatenate(
-        [
-            jnp.einsum("d,rde->re", own_part[0], mod_weight, preferred_element_type=jnp.float32),
-            jnp.einsum(
-                "d,rde->re", own_part[1], mod_weight[:2], preferred_element_type=jnp.float32
-            ),
+    vmem = pl.BlockSpec(memory_space=pltpu.VMEM)
+    smem = pl.BlockSpec(memory_space=pltpu.SMEM)
+    copies = len(ITEM_ORDER) + 16 + 8 + 2 + 32 + 2 + 16 + 3 * 16
+    base, table = rotation_tables()
+    row = lambda v: v.reshape(1, -1)
+    return pl.pallas_call(
+        whole_kernel,
+        out_shape=jax.ShapeDtypeStruct((64, D), BF),
+        in_specs=[vmem] * 16 + [smem] + [vmem] * 3,
+        out_specs=vmem,
+        scratch_shapes=[
+            pltpu.VMEM((8, 128, 768), BF),
+            pltpu.VMEM((8, 128, 512), BF),
+            pltpu.VMEM((64, D), BF),
+            pltpu.VMEM((16, 8, 128), F32),
+            pltpu.VMEM((16, 8, 128), F32),
+            pltpu.VMEM((16, 160, 128), BF),
+            pltpu.VMEM((160, 768), F32),
+            pltpu.VMEM((160, 512), F32),
+            pltpu.VMEM((64, 768), F32),
+            pltpu.VMEM((96, 512), F32),
+            pltpu.VMEM((16, 64, 768), BF),
+            pltpu.VMEM((16, 64, 640), BF),
+            pltpu.VMEM((128, 768), BF),
+            pltpu.VMEM((160, 640), BF),
+            pltpu.VMEM((768, 128), F32),
+            pltpu.VMEM((128, 1024), BF),
+            pltpu.VMEM((N_UNITS, 2, HEAD + VDIM, 256), BF),
+            pltpu.VMEM((16, CTX_DEV, 256), BF),
+            pltpu.VMEM((8, 64, D // 2), BF),
+            pltpu.VMEM((8, 64, D // 2), BF),
+            pltpu.VMEM((512, 1024), F32),
+            pltpu.VMEM((512, 1024), F32),
+            pltpu.VMEM((1, 1024), F32),
+            pltpu.VMEM((1, 1024), F32),
+            pltpu.VMEM((1, 1024), F32),
+            pltpu.VMEM((1, 1024), F32),
+            pltpu.VMEM((VDIM, 1024), F32),
+            pltpu.VMEM((8, VDIM, 128), BF),
+            pltpu.VMEM((8, VDIM, 128), BF),
+            pltpu.VMEM((128, D), F32),
+            pltpu.VMEM((64, D), F32),
+            pltpu.SemaphoreType.DMA((copies,)),
+            pltpu.SemaphoreType.DMA((copies,)),
         ],
-        axis=0,
-    )
-    summed = lax.psum(partial_value, "sp")
-    modulations = lax.all_gather(summed, "tp", axis=1, tiled=True)
-    normed = modulate(latent, norm_gain, modulations[0], modulations[1])
-    context_normed = modulate(context, norm_gain, modulations[3], modulations[4])
-    stacked = jnp.concatenate([normed, context_normed], axis=0)
-    pieces = sent_together((down_q, down_kv), "tp", 0, 1)
-    query_down = jnp.dot(stacked[:own_rows], pieces[0], preferred_element_type=jnp.float32)
-    kv_down = jnp.dot(stacked, pieces[1], preferred_element_type=jnp.float32)
-    query_latent = rms_scale(query_down, qlat_gain).astype(jnp.bfloat16)
-    kv_latent = rms_scale(kv_down, kvlat_gain).astype(jnp.bfloat16)
-    rope_rows = jnp.dot(stacked, rope_weight, preferred_element_type=jnp.float32).astype(
-        jnp.bfloat16
-    )
-    all_query, all_kv, all_rope = sent_together(
-        (query_latent, kv_latent[:own_rows], rope_rows[:own_rows]), "tp", 0, 1
-    )
-    ck, cv = make_keys(
-        kv_latent[own_rows:], rope_rows[own_rows:], up_key, up_value, key_gain, None
-    )
-    positions = seq_index * block_tokens + jnp.arange(block_tokens, dtype=jnp.int32)
-    tables = axial_tables(positions)
-    queries = make_queries(all_query, up_query, query_gain, tables)
-    keys, values = make_keys(all_kv, all_rope, up_key, up_value, key_gain, tables)
-    qt = jnp.pad(queries, ((0, 0), (0, 128 - HEAD))).T
-    kvt = jnp.concatenate([keys, values], axis=1).T
-    kvt = kvt.reshape(HEAD + VDIM, 2, 2, 256).transpose(1, 2, 0, 3)
-    ctx = jnp.concatenate(
-        [jnp.pad(ck, ((0, 0), (0, 128 - HEAD))), jnp.pad(cv, ((0, 0), (0, 128 - VDIM)))], axis=1
-    )
-    gates = modulations[2:3]
-    return attention(qt, kvt, ctx, context_bias.reshape(1, 1), out_weight, latent, gates)
+        compiler_params=pltpu.CompilerParams(collective_id=0, has_side_effects=True,
+                                             vmem_limit_bytes=56 * 1024 * 1024),
+        name="whole",
+    )(latent, context, row(cond), row(cond_context), mod_weight, row(norm_gain), down_q, down_kv,
+      rope_weight, row(qlat_gain), row(kvlat_gain), up_query, up_key, up_value, row(query_gain),
+      row(key_gain), context_bias.reshape(1, 1), out_weight, jnp.asarray(base),
+      jnp.asarray(table))
 
 
 def solution(mesh):

time: 190 us -> 123 us (0.65)
  blocking collectives: 62.1 us -> 0 us
  Pallas kernels: 54 us -> 112 us
  waiting for transfers between devices: 32.3 us -> 0 us
  between operations: 14.4 us -> 0.69 us
  matrix products: 12.1 us -> 0 us
  other arithmetic: 10.8 us -> 0 us
  local copies, waits for them, and re-layouts: 3.71 us -> 9.82 us
    pallas_call x1, Pallas kernels: 54 us -> 112 us  [shards(): pl.pallas_call(whole_kernel, out_shape=jax.ShapeDtypeStruct((64, D), BF),...]
    psum x1 -> x0, blocking collectives: 34.2 us -> none  [shards(): summed = lax.psum(partial_value, 'sp')]
    all_gather x2 -> x0, waiting for transfers between devices: 32.2 us -> none  [sent_together(): lax.all_gather(both, axis, axis=dim, tiled=True)]
    all_gather x1 -> x0, blocking collectives: 27.9 us -> none  [shards(): modulations = lax.all_gather(summed, 'tp', axis=1, tiled=True)]
    dot_general x10 -> x0, matrix products: 12.1 us -> none  [the longest x1 2.63 us: shards(): jnp.dot(stacked[:own_rows], pieces[0], preferred_element_type=jnp.float32)]
    unnamed x20 -> x21, local copies, waits for them, and re-layouts: 0.9 us -> 6.83 us
    convert_element_type x14 -> x0, other arithmetic: 4.55 us -> none  [the longest x2 2.15 us: modulate(): return (normal * (1.0 + scales) + shifts).astype(jnp.bfloat16)]
    reshape x2 -> x5, local copies, waits for them, and re-layouts: 0.27 us -> 2.99 us  [shards(): row = lambda v: v.reshape(1, -1)]
  transfers between devices with their start and end apart: 2 -> 0, of which waited for: 1 -> 0; matrix products, arithmetic and copies ran while one was open for 6% -> 0% of each run, Pallas kernels for 0% -> 0%
where the time goes in v2:
time: 123 us
  Pallas kernels  112 us (91%)
  local copies, waits for them, and re-layouts  9.82 us (8%)
    pallas_call x1, Pallas kernels, shards(): pl.pallas_call(whole_kernel, out_shape=jax.ShapeDtypeStruct((64, D), BF),...  112 us
    unnamed x21, local copies, waits for them, and re-layouts  6.83 us
    reshape x5, local copies, waits for them, and re-layouts, shards(): row = lambda v: v.reshape(1, -1)  2.99 us

profile of v2, /device:TPU:1, one launch (start us, length us, event | category | flops | bytes accessed | tf_op | source)
XLA Modules:
  0.0 122.8 jit_solution(2154772938143547401)
XLA Ops:
  0.7 0.0 copy-start.7
  0.7 0.0 copy-start.6
  0.7 0.7 copy-done.7
  1.3 0.0 copy-start.3
  1.3 0.6 reshape.28.kvlg_ref
  1.9 0.0 copy-done.6
  1.9 0.6 reshape.27.qlg_ref
  2.5 0.0 copy-done.3
  2.5 0.0 copy-start.4
  2.5 0.6 reshape.24.cond_ref
  3.1 0.1 copy-done.4
  3.2 0.0 copy-start.5
  3.2 0.6 reshape.25.condc_ref
  3.8 0.1 copy-done.5
  3.9 0.0 copy-start.2
  3.9 0.6 reshape.26.ng_ref
  4.5 0.0 copy-start
  4.5 1.6 %copy.23.upk_ref = bf16[512,64]{1,0:T(8,128)(2,1)} copy(bf16[512,64]{0,1:T(8,128)(2,1)} %param.32) | data formatting | bytes 131072 | tf_op args[12]
  6.2 0.0 copy-done.2
  6.2 0.8 copy.24.upv_ref
  6.9 0.0 copy-done
  6.9 0.0 copy-start.1
  6.9 0.8 copy.22.upq_ref
  7.7 0.1 copy-done.1
  7.8 1.0 copy.21.rw_ref
  8.8 112.3 %whole.1 = bf16[64,2048]{1,0:T(8,128)(2,1)} custom-call(bf16[64,2048]{1,0:T(8,128)(2,1)} %lat_ref.1, bf16[32,2048]{1,0:T(8,128)(2,1)} %context_ref.1, bf16[1,2048]{1,0:T(2,128)(2,1)} %reshape.24.cond_ref, bf16[1,2048]{1,0:T(2,128)(2,1)} %reshape.25.condc_ref, bf16[3,128,128]{2,1,0:T(8,128)(2,1)} %mw_ref.1, bf16[1,2048]{1,0:T(2,128)(2,1)} %reshape.26.ng_ref, ...), custom_call_target="tpu_custom_call" | custom-call | tf_op jit(solution)/shard_map/whole/pallas_call | solution.py:614
  121.1 1.7 %copy.27 = bf16[64,2048]{1,0:T(8,128)(2,1)} copy(bf16[64,2048]{1,0:T(8,128)(2,1)} %whole.1) | data formatting | bytes 524288
Async XLA Ops:
  0.7 0.7 copy-start.7
  0.7 1.3 %copy-start.6 = (bf16[768]{0:T(1024)(128)(2,1)S(1)}, bf16[768]{0:T(1024)(128)(2,1)}, u32[]{:S(2)}) copy-start(bf16[768]{0:T(1024)(128)(2,1)} %param.29) | copy-start | bytes 4612
  1.3 1.2 copy-start.3
  2.5 0.7 copy-start.4
  3.2 0.7 copy-start.5
  3.9 2.3 %copy-start.2 = (bf16[512,64]{0,1:T(8,128)(2,1)S(1)}, bf16[512,64]{0,1:T(8,128)(2,1)}, u32[]{:S(2)}) copy-start(bf16[512,64]{0,1:T(8,128)(2,1)} %param.33) | copy-start | bytes 196612
  4.5 2.4 %copy-start = (bf16[768,96]{0,1:T(8,128)(2,1)S(1)}, bf16[768,96]{0,1:T(8,128)(2,1)}, u32[]{:S(2)}) copy-start(bf16[768,96]{0,1:T(8,128)(2,1)} %param.31) | copy-start | bytes 442372
  6.9 0.9 copy-start.1

commit v3 on v2

--- a/solution.py
+++ b/solution.py
@@ -50,68 +50,85 @@
     return items
 
 
-def arrival_times(items, unit=3.53, latency=1.8):
+RELEASE = (10.0, 17.5)
+EARLY_AT = 16.0
+LOOP_AT = 19.5
+STEP = 0.78
+UNIT, LATENCY = 3.53, 1.9
+
+
+def plan_exchange(items):
     free, arrive = {}, {}
-    waiting = []
-    for n, (key, (axis, step, trigger)) in enumerate(items.items()):
-        if trigger is None:
-            first = axis == ("x" if key[0] == 0 else "y")
-            waiting.append((0.0, 0 if first else 1, n, key))
-    count = len(items)
-    while waiting:
-        waiting.sort()
-        at, _, _, key = waiting.pop(0)
+    left = dict(items)
+
+    def send(key, at):
         axis, step, _ = items[key]
-        span = unit if key[3] == "U" else unit / 2
         begin = max(at, free.get((axis, step), 0.0))
-        free[(axis, step)] = begin + span
-        arrive[key] = begin + span + latency
-        for other, (_, _, trigger) in items.items():
-            if trigger == key:
-                count += 1
-                waiting.append((arrive[key], 0, count, other))
-    return arrive
+        free[(axis, step)] = begin + (UNIT if key[3] == "U" else UNIT / 2)
+        arrive[key] = free[(axis, step)] + LATENCY
+
+    def begin_half(h, at):
+        keys = [k for k in items if items[k][2] is None and k[0] == h]
+        first = "x" if h == 0 else "y"
+        for key in sorted(keys, key=lambda k: 0 if items[k][0] == first else 1):
+            send(key, at)
+
+    taken = []
+
+    def rank(key):
+        return (round(arrive[key], 1), 0 if key[2] == 0 else 1, str(key))
+
+    def take(now, limit=None):
+        got = []
+        while True:
+            here = sorted((k for k in arrive if k not in taken and arrive[k] <= now), key=rank)
+            if not here or (limit is not None and len(got) >= limit):
+                return got
+            key = here[0]
+            taken.append(key)
+            got.append(key)
+            for other in items:
+                if items[other][2] == key:
+                    send(other, now)
+
+    begin_half(0, RELEASE[0])
+    early = take(EARLY_AT, 3)
+    begin_half(1, RELEASE[1])
+    now = LOOP_AT
+    units = [(0, 0, 0), (1, 0, 0)]
+    every = sorted({k[:3] for k in items})
+
+    def ready():
+        done = [u for u in every if u not in units
+                and all(k in taken for k in items if k[:3] == u)]
+        return sorted(done, key=lambda u: (max(arrive[k] for k in items if k[:3] == u), str(u)))
+
+    plan = [take(now)]
+    for n in range(1, len(every) + 3, 2):
+        got = take(now)
+        while len(units) < min(n + 2, len(every) + 2):
+            come = ready()
+            if come:
+                units.append(come[0])
+                continue
+            now = min(arrive[k] for k in arrive if k not in taken)
+            got = got + take(now)
+        plan.append(got)
+        now += 2 * STEP
+    return early, plan, units, now
 
 
 ITEMS = exchange_items()
-ARRIVE = arrival_times(ITEMS)
-ITEM_ORDER = sorted(ITEMS, key=lambda k: (round(ARRIVE[k], 1), str(k)))
+EARLY, PLAN, UNITS, PLAN_END = plan_exchange(ITEMS)
+ITEM_ORDER = list(ITEMS)
 ITEM_INDEX = {k: n for n, k in enumerate(ITEM_ORDER)}
-
-
-def unit_order():
-    ready = {}
-    for k in ITEM_ORDER:
-        ready[k[:3]] = max(ready.get(k[:3], 0.0), ARRIVE[k])
-    units = sorted(ready, key=lambda u: (round(ready[u], 1), str(u)))
-    return [(0, 0, 0), (1, 0, 0)] + units
-
-
-UNITS = unit_order()
 SLOT = {u: n for n, u in enumerate(UNITS)}
 N_UNITS = len(UNITS) + 1
 CTX_SLOT = len(UNITS)
 
 
-def item_steps(per_step=0.62):
-    steps = {}
-    now = 0.0
-    placed = set()
-    plan = []
-    for n in range(N_UNITS):
-        need = []
-        if n < len(UNITS):
-            need = [k for k in ITEM_ORDER if k[:3] == UNITS[n] and k not in placed]
-        for k in need:
-            now = max(now, ARRIVE[k])
-        early = [k for k in ITEM_ORDER if k not in placed and (k in need or ARRIVE[k] <= now)]
-        placed.update(early)
-        plan.append(early)
-        now += per_step
-    return plan
-
-
-PLAN = item_steps()
+def mark(name):
+    pass
 
 
 class Board:
@@ -197,9 +214,12 @@
 
     def begin(self):
         for part in (0, 1):
-            for way in (1, -1):
-                self.board.send(self.number(way, 1, part), self.own[part],
-                                self.bufs[part].at[self.index(0)], self.place.ring(way))
+            self.begin_part(part)
+
+    def begin_part(self, part):
+        for way in (1, -1):
+            self.board.send(self.number(way, 1, part), self.own[part],
+                            self.bufs[part].at[self.index(0)], self.place.ring(way))
 
     def take(self, way, dist, part):
         here = self.slot(way, dist, part)
@@ -236,7 +256,7 @@
 def whole_kernel(lat_ref, context_ref, cond_ref, condc_ref, mw_ref, ng_ref, dq_ref, dkv_ref,
                  rw_ref, qlg_ref, kvlg_ref, upq_ref, upk_ref, upv_ref, qg_ref, kg_ref, bias_ref,
                  ow_ref, base_ref, tab_ref, out_ref,
-                 wq, wkv, latsib, modp, modf, xn, uq, ukv, sq, skv, lq, lk, upt, wk, pad,
+                 wq, wkv, latsib, modp, modf, xn, uq, ukv, sq, skv, lq, lk, wk, rt,
                  qt, kvb, cbuf, owa, owb, s_a, s_b, mb_a, mb_b, m_ref, l_ref, acc, att, attb,
                  part_ref, sib_ref, sends, recvs):
     place = Place()
@@ -253,21 +273,22 @@
     half_cols = D // 2
     ring = ZRing(board, place, (ow_ref.at[:, :half_cols], ow_ref.at[:, half_cols:]), (owa, owb))
     wring = ZRing(board, place, (dq_ref, dkv_ref), (wq, wkv))
-    lring = ZRing(board, place, (lq.at[place.t], lk.at[place.t]), (lq, lk), by_device=True)
-
+    lring = ZRing(board, place, (lk.at[place.t], lq.at[place.t]), (lk, lq), by_device=True)
+
+    mark("a_greet")
     greet([place.sp_peer(k) for k in range(1, 16)] + [place.tp_peer(k) for k in range(1, 16)])
 
+    mark("b_mod")
     wring.begin()
     board.send(lat_d2d, lat_ref, latsib, place.sibling())
 
-    span = pl.ds(pl.multiple_of(place.s * 128, 128), 128)
-
-    def silu(v):
-        v = v.astype(F32)
+    def silu(ref):
+        rows = lax.broadcasted_iota(jnp.int32, (16, 128), 0)
+        v = jnp.sum(jnp.where(rows == place.s, ref[...].astype(F32), 0.0), axis=0, keepdims=True)
         return v / (1.0 + jnp.exp(-v))
 
     act = jnp.concatenate(
-        [silu(cond_ref[:, span]), silu(condc_ref[:, span]), jnp.zeros((14, 128), F32)],
+        [silu(cond_ref), silu(condc_ref), jnp.zeros((14, 128), F32)],
         axis=0).astype(BF)
     terms = [jnp.dot(act, mw_ref[r], preferred_element_type=F32) for r in range(3)]
     modp[place.s] = jnp.concatenate(
@@ -276,19 +297,14 @@
     for k in range(1, 16):
         board.send(modp_base + k, modp.at[place.s], modp.at[place.s], place.sp_peer(k))
 
+    mark("c_local")
     wq[place.z] = dq_ref[...]
     wkv[place.z] = dkv_ref[...]
     owa[place.z] = ow_ref[:, :half_cols]
     owb[place.z] = ow_ref[:, half_cols:]
-    pad[...] = jnp.zeros(pad.shape, F32)
-    pad[:, 0:HEAD] = upq_ref[...].astype(F32)
-    upt[...] = pad[...].T.astype(BF)
     wk[...] = jnp.zeros(wk.shape, BF)
-    pad[0:512, 0:NOPE] = upk_ref[...].astype(F32)
-    pad[0:512, NOPE:128] = upv_ref[...].astype(F32)
-    turned_up = pad[0:512, :].T.astype(BF)
-    wk[0:NOPE, 0:512] = turned_up[0:NOPE]
-    wk[HEAD:HEAD + VDIM, 0:512] = turned_up[NOPE:128]
+    wk[0:NOPE, 0:512] = upk_ref[...]
+    wk[HEAD:HEAD + VDIM, 0:512] = upv_ref[...]
     unit = (lax.broadcasted_iota(jnp.int32, (ROPE, 128), 0)
             == lax.broadcasted_iota(jnp.int32, (ROPE, 128), 1))
     wk[NOPE:HEAD, 512:640] = jnp.where(unit, 1.0, 0.0).astype(BF)
@@ -300,6 +316,7 @@
     inv_own = inverse(lat_ref)
     inv_ctx = inverse(context_ref)
 
+    mark("d_modwait")
     for k in range(1, 16):
         board.arrived(modp_base + k, modp.at[(place.s - k + 16) % 16], place.sp_peer(16 - k))
     modf[place.t] = jnp.sum(modp[...], axis=0)
@@ -311,12 +328,15 @@
     w_items = wring.items()
     for item in w_items[:4]:
         wring.take(*item)
+    mark("e_modfwait")
     for k in range(1, 16):
         board.arrived(modf_base + k, modf.at[(place.t - k + 16) % 16], place.tp_peer(16 - k))
 
+    mark("f_norm")
+    norm_gain = ng_ref[...].astype(F32)
     for k in range(16):
         cols = slice(k * 128, (k + 1) * 128)
-        gain = ng_ref[:, cols].astype(F32)
+        gain = norm_gain[k:k + 1]
         shift, scale = modf[k, 0:1, :], modf[k, 1:2, :]
         own = lat_ref[:, cols].astype(F32) * inv_own * gain
         xn[k, 0:64] = (own * (1.0 + scale) + shift).astype(BF)
@@ -334,40 +354,46 @@
 
     uq[...] = jnp.dot(xn[place.t], wq[place.z], preferred_element_type=F32)
     ukv[...] = jnp.dot(xn[place.t], wkv[place.z], preferred_element_type=F32)
-    rope = jnp.dot(xn[0, 0:96], rw_ref[0:128], preferred_element_type=F32)
-    for k in range(1, 16):
-        rope = rope + jnp.dot(xn[k, 0:96], rw_ref[k * 128:(k + 1) * 128],
-                              preferred_element_type=F32)
+    contract = (((1,), (1,)), ((), ()))
+    rope = jnp.zeros((96, ROPE), F32)
+    for k in range(16):
+        rope = rope + lax.dot_general(xn[k, 0:96], rw_ref[:, k * 128:(k + 1) * 128], contract,
+                                      preferred_element_type=F32)
     rope = rope.astype(BF).astype(F32)
+    mark("g_wring")
     for n, (way, dist, part) in enumerate(w_items):
         if n >= 4:
             wring.take(way, dist, part)
         add_product(wring.index(way * dist), part)
 
+    mark("h_d2dpart")
+    board.send(part_base + 1, ukv.at[64:160], skv, place.sibling())
     board.send(part_base, uq.at[96:160], sq, place.sibling())
-    board.send(part_base + 1, ukv.at[64:160], skv, place.sibling())
 
     def latent_of(total, gain_ref):
+        gain = gain_ref[...].astype(F32)
+        gain = jnp.concatenate([gain[k:k + 1] for k in range(gain.shape[0])], axis=1)
         return (total * lax.rsqrt(jnp.mean(total * total, axis=-1, keepdims=True) + epsilon)
-                * gain_ref[...].astype(F32)).astype(BF)
-
-    board.arrived(part_base, sq, place.sibling())
-    lq[place.t] = latent_of(uq[0:64] + sq[...], qlg_ref)
+                * gain).astype(BF)
+
     board.arrived(part_base + 1, skv, place.sibling())
     lk[place.t, :, 0:512] = latent_of(ukv[0:64] + skv[32:96], kvlg_ref)
     lk[place.t, :, 512:640] = jnp.concatenate(
         [rope[0:64], jnp.zeros((64, 96), F32)], axis=1).astype(BF)
-    lring.begin()
-
     def share(number, ref):
         board.send(share_base + number, ref, ref, place.sibling())
 
-    share(0, lq.at[place.t])
-    share(1, lk.at[place.t])
-
+    lring.begin_part(0)
+    share(0, lk.at[place.t])
+    board.arrived(part_base, sq, place.sibling())
+    lq[place.t] = latent_of(uq[0:64] + sq[...], qlg_ref)
+    lring.begin_part(1)
+    share(1, lq.at[place.t])
+
+    mark("i_ctx")
     ctx_kv = latent_of(ukv[64:96] + skv[0:32], kvlg_ref)
-    ctx_k = jnp.dot(ctx_kv, upk_ref[...], preferred_element_type=F32)
-    ctx_v = jnp.dot(ctx_kv, upv_ref[...], preferred_element_type=F32)
+    ctx_k = lax.dot_general(ctx_kv, upk_ref[...], contract, preferred_element_type=F32)
+    ctx_v = lax.dot_general(ctx_kv, upv_ref[...], contract, preferred_element_type=F32)
     ctx_u = jnp.concatenate([ctx_k, rope[64:96]], axis=1)
     ctx_n = ctx_u * lax.rsqrt(jnp.mean(ctx_u * ctx_u, axis=-1, keepdims=True) + epsilon)
     ctx_n = ctx_n * kg_ref[...]
@@ -379,15 +405,17 @@
 
     base = base_ref[pl.ds(pl.multiple_of(place.s * 16, 16), 16)]
     base_cos, base_sin = base[0:8, 0:1], base[8:16, 0:1]
-    row_cos = tab_ref[0:8] * base_cos - tab_ref[8:16] * base_sin
-    row_sin = tab_ref[8:16] * base_cos + tab_ref[0:8] * base_sin
-    col_cos, col_sin = tab_ref[16:24], tab_ref[24:32]
+    rt[0:8] = tab_ref[0:8] * base_cos - tab_ref[8:16] * base_sin
+    rt[8:16] = tab_ref[8:16] * base_cos + tab_ref[0:8] * base_sin
+    rt[16:32] = tab_ref[16:32]
 
     def column(gain_ref):
         row = jnp.concatenate([gain_ref[...], jnp.zeros((1, 128 - HEAD), F32)], axis=1)
         return jnp.broadcast_to(row, (128, 128)).T[0:HEAD, 0:1]
 
-    def turned(u, gain):
+    def turned(u, gain, cols):
+        row_cos, row_sin = rt[0:8, cols], rt[8:16, cols]
+        col_cos, col_sin = rt[16:24, cols], rt[24:32, cols]
         normal = u * lax.rsqrt(jnp.mean(u * u, axis=0, keepdims=True) + epsilon) * gain
         a, b, c, d = (normal[NOPE + 8 * n:NOPE + 8 * n + 8] for n in range(4))
         return jnp.concatenate(
@@ -395,33 +423,6 @@
              c * col_cos - d * col_sin, d * col_cos + c * col_sin], axis=0)
 
     query_gain, key_gain = column(qg_ref), column(kg_ref)
-
-    own_at = [(1, 0), (-1, 0)]
-    for n, (way, dist, part) in enumerate(lring.items()):
-        lring.take(way, dist, part)
-        share(2 + n, lring.slot(way, dist, part))
-    other = 1 - place.c
-    for part, buf in enumerate((lq, lk)):
-        board.arrived(share_base + part, buf.at[place.z * 2 + other], place.sibling())
-    for n, (way, dist, part) in enumerate(lring.items()):
-        at = ((place.z - way * dist + 16) % 8) * 2 + other
-        board.arrived(share_base + 2 + n, (lq, lk)[part].at[at], place.sibling())
-
-    contract = (((1,), (1,)), ((), ()))
-    kv = lax.dot_general(wk[...], lk[...].reshape(1024, 640), contract,
-                         preferred_element_type=F32)
-    kv = jnp.concatenate([turned(kv[0:HEAD], key_gain), kv[HEAD:HEAD + VDIM]],
-                         axis=0).astype(BF)
-    for h in (0, 1):
-        for q in (0, 1):
-            at = (2 * h + q) * 256
-            kvb[SLOT[(h, 0, 0)], q] = kv[:, at:at + 256]
-
-    def queries():
-        u = lax.dot_general(upt[...], lq[...].reshape(1024, 768), contract,
-                            preferred_element_type=F32)
-        qt[0:HEAD] = turned(u[0:HEAD], query_gain).astype(BF)
-        qt[HEAD:128] = jnp.zeros((128 - HEAD, 1024), BF)
 
     def finish():
         wring.drain()
@@ -432,9 +433,9 @@
             board.sent(modf_base + k, modf.at[place.t], place.tp_peer(k))
         board.sent(part_base, uq.at[96:160], place.sibling())
         board.sent(part_base + 1, ukv.at[64:160], place.sibling())
-        share_sizes = [0, 1] + [item[2] for item in lring.items()]
+        share_sizes = [0, 1] + [item[2] for item in l_items]
         for n, part in enumerate(share_sizes):
-            board.sent(share_base + n, (lq, lk)[part].at[0], place.sibling())
+            board.sent(share_base + n, (lk, lq)[part].at[0], place.sibling())
 
     def kv_send(key, src):
         axis, step, _ = ITEMS[key]
@@ -445,11 +446,10 @@
     def own_part(h):
         return kvb.at[SLOT[(h, 0, 0)]]
 
-    for key in sorted((k for k in ITEMS if ITEMS[k][2] is None),
-                      key=lambda k: 0 if ITEMS[k][0] == ("x" if k[0] == 0 else "y") else 1):
-        kv_send(key, own_part(key[0]))
-    ring.begin()
-    queries()
+    def kv_begin(h):
+        for key in sorted((k for k in ITEMS if ITEMS[k][2] is None and k[0] == h),
+                          key=lambda k: 0 if ITEMS[k][0] == ("x" if k[0] == 0 else "y") else 1):
+            kv_send(key, own_part(h))
 
     def kv_take(key):
         axis, step, _ = ITEMS[key]
@@ -462,6 +462,79 @@
                     src = kvb.at[SLOT[key[:3]], other[3]]
                 kv_send(other, src)
 
+    mark("j_lring")
+    l_items = lring.items()
+    other = 1 - place.c
+
+    def ring_take(way, dist, part):
+        lring.take(way, dist, part)
+        share(2 + l_items.index((way, dist, part)), lring.slot(way, dist, part))
+
+    def chip(dist, part):
+        at = (place.z - dist + 16) % 8
+        if dist == 0:
+            number = part
+        elif dist == 4:
+            number = 2 + l_items.index((1 if part == 0 else -1, 4, part))
+        else:
+            number = 2 + l_items.index((1 if dist > 0 else -1, abs(dist), part))
+        buf = (lk, lq)[part]
+        board.arrived(share_base + number, buf.at[at * 2 + other], place.sibling())
+        cols = pl.ds(pl.multiple_of(at * 128, 128), 128)
+        return buf[pl.ds(at * 2, 2)].reshape(128, buf.shape[2]), cols
+
+    def chip_keys(dist, h, n):
+        rows, cols = chip(dist, 0)
+        kv = lax.dot_general(wk[...], rows, contract, preferred_element_type=F32)
+        kv = jnp.concatenate([turned(kv[0:HEAD], key_gain, cols), kv[HEAD:HEAD + VDIM]], axis=0)
+        kvb[SLOT[(h, 0, 0)], n // 2, :, (n % 2) * 128:(n % 2) * 128 + 128] = kv.astype(BF)
+
+    def chip_queries(dist):
+        rows, cols = chip(dist, 1)
+        u = lax.dot_general(upq_ref[...], rows, contract, preferred_element_type=F32)
+        qt[0:HEAD, cols] = turned(u, query_gain, cols).astype(BF)
+
+    qt[HEAD:128] = jnp.zeros((128 - HEAD, 1024), BF)
+    ring_take(1, 1, 0)
+    ring_take(-1, 1, 0)
+    chip_keys(0, 0, 0)
+    ring_take(1, 1, 1)
+    ring_take(-1, 1, 1)
+    chip_keys(1, 0, 1)
+    chip_keys(-1, 0, 2)
+    ring_take(1, 2, 0)
+    ring_take(-1, 2, 0)
+    chip_queries(0)
+    chip_keys(2, 0, 3)
+    mark("k_h0")
+    kv_begin(0)
+    ring_take(1, 2, 1)
+    ring_take(-1, 2, 1)
+    chip_queries(1)
+    chip_queries(-1)
+    ring_take(1, 3, 0)
+    ring_take(-1, 3, 0)
+    chip_keys(-2, 1, 0)
+    chip_queries(2)
+    ring_take(1, 3, 1)
+    ring_take(-1, 3, 1)
+    ring.begin()
+    chip_keys(3, 1, 1)
+    chip_keys(-3, 1, 2)
+    chip_queries(-2)
+    mark("l_early")
+    for key in EARLY:
+        kv_take(key)
+    mark("l_h1")
+    ring_take(1, 4, 0)
+    chip_keys(4, 1, 3)
+    kv_begin(1)
+    mark("l_q")
+    chip_queries(3)
+    chip_queries(-3)
+    ring_take(-1, 4, 1)
+    chip_queries(4)
+
     def ctx_unit():
         for k in range(1, 16):
             board.arrived(ctx_base + k, cbuf.at[(place.s - k + 16) % 16], place.sp_peer(16 - k))
@@ -470,6 +543,7 @@
             kvb[CTX_SLOT, q, 0:HEAD, :] = turned[0:HEAD, q * 256:(q + 1) * 256]
             kvb[CTX_SLOT, q, HEAD:HEAD + VDIM, :] = turned[128:128 + VDIM, q * 256:(q + 1) * 256]
 
+    mark("m_init")
     m_ref[...] = jnp.full(m_ref.shape, -jnp.inf, F32)
     l_ref[...] = jnp.zeros(l_ref.shape, F32)
     acc[...] = jnp.zeros(acc.shape, F32)
@@ -505,42 +579,34 @@
             acc[:, cols] = acc[:, cols] * factor + summed
 
     ring_items = ring.items()
-    ring_plan = [[] for _ in range(N_UNITS)]
+    ring_plan = [[] for _ in range(17)]
     for n, item in enumerate(ring_items):
-        ring_plan[min(4 + (n * 26) // len(ring_items), N_UNITS - 1)].append(item)
+        ring_plan[min(2 + (n * 13) // len(ring_items), 16)].append(item)
 
     def actions(n):
         for key in PLAN[n]:
             kv_take(key)
         for item in ring_plan[n]:
             ring.take(*item)
-        if n == CTX_SLOT:
-            ctx_unit()
-
-    def act_in_loop(i, offset):
-        for trip in range(16):
-            n = 2 * trip + offset
-            if PLAN[n] or ring_plan[n] or n == CTX_SLOT:
-                @pl.when(i == trip)
-                def _():
-                    actions(n)
-
+
+    mark("n_prolog")
     actions(0)
     products(0, s_a, mb_a)
-
-    def body(i, carry):
-        act_in_loop(i, 1)
+    for i in range(16):
+        mark(f"o{i:02d}a")
+        actions(i + 1)
+        if i == 15:
+            ctx_unit()
+        mark(f"o{i:02d}b")
         products(2 * i + 1, s_b, mb_b)
         absorb(2 * i, s_a, mb_a, None)
-        act_in_loop(i, 2)
         products(2 * i + 2, s_a, mb_a)
         absorb(2 * i + 1, s_b, mb_b, None)
-        return carry
-
-    lax.fori_loop(0, 16, body, 0)
+    mark("p_last")
     bias = (bias_ref[0, 0] + math.log(TOK_DEV / CTX_DEV)) * LOG2E
     absorb(CTX_SLOT, s_a, mb_a, bias)
 
+    mark("q_a2a")
     for k in range(8):
         cols = slice(k * 128, (k + 1) * 128)
         att[k] = (acc[:, cols] / l_ref[:, cols]).astype(BF)
@@ -549,11 +615,13 @@
     attb[place.z] = att[place.z]
     for k in range(1, 8):
         board.arrived(a2a_base + k, attb.at[(place.z - k + 8) % 8], place.ring(-k))
+    mark("r_out")
     rows = attb[...].reshape(8 * VDIM, 128).astype(F32).T.astype(BF)
     for n, weight in enumerate((owa, owb)):
         part_ref[:, n * half_cols:(n + 1) * half_cols] = jnp.dot(
             rows, weight[...].reshape(8 * VDIM, half_cols), preferred_element_type=F32)
     away = part_ref.at[pl.ds(pl.multiple_of(64 * (1 - place.c), 64), 64)]
+    mark("s_d2d")
     board.send(d2d, away, sib_ref, place.sibling())
     board.arrived(d2d, sib_ref, place.sibling())
     gates = jnp.concatenate([modf[k, 2:3, :] for k in range(16)], axis=1)
@@ -561,6 +629,7 @@
     projected = mine + sib_ref[...]
     out_ref[...] = (lat_ref[...].astype(F32) + gates * projected).astype(BF)
 
+    mark("t_drain")
     board.sent(d2d, away, place.sibling())
     for k in range(1, 8):
         board.sent(a2a_base + k, att.at[(place.z + k) % 8], place.ring(k))
@@ -572,6 +641,7 @@
         axis, step, _ = ITEMS[key]
         src = quarter_ref(kvb, 0, key[3])
         board.sent(kv_base + ITEM_INDEX[key], src, place.plane(axis, step))
+    mark(None)
 
 
 def rotation_tables():
@@ -611,6 +681,7 @@
     copies = len(ITEM_ORDER) + 16 + 8 + 2 + 32 + 2 + 16 + 3 * 16
     base, table = rotation_tables()
     row = lambda v: v.reshape(1, -1)
+    fold = lambda v: v.reshape(-1, 128)
     return pl.pallas_call(
         whole_kernel,
         out_shape=jax.ShapeDtypeStruct((64, D), BF),
@@ -629,9 +700,8 @@
             pltpu.VMEM((96, 512), F32),
             pltpu.VMEM((16, 64, 768), BF),
             pltpu.VMEM((16, 64, 640), BF),
-            pltpu.VMEM((128, 768), BF),
             pltpu.VMEM((160, 640), BF),
-            pltpu.VMEM((768, 128), F32),
+            pltpu.VMEM((ROPE, 1024), F32),
             pltpu.VMEM((128, 1024), BF),
             pltpu.VMEM((N_UNITS, 2, HEAD + VDIM, 256), BF),
             pltpu.VMEM((16, CTX_DEV, 256), BF),
@@ -654,8 +724,8 @@
         compiler_params=pltpu.CompilerParams(collective_id=0, has_side_effects=True,
                                              vmem_limit_bytes=56 * 1024 * 1024),
         name="whole",
-    )(latent, context, row(cond), row(cond_context), mod_weight, row(norm_gain), down_q, down_kv,
-      rope_weight, row(qlat_gain), row(kvlat_gain), up_query, up_key, up_value, row(query_gain),
+    )(latent, context, fold(cond), fold(cond_context), mod_weight, fold(norm_gain), down_q, down_kv,
+      rope_weight.T, fold(qlat_gain), fold(kvlat_gain), up_query.T, up_key.T, up_value.T, row(query_gain),
       row(key_gain), context_bias.reshape(1, 1), out_weight, jnp.asarray(base),
       jnp.asarray(table))
 

time: 123 us -> 111 us (0.902)
  local copies, waits for them, and re-layouts: 9.82 us -> 1.67 us
  Pallas kernels: 112 us -> 109 us
    unnamed x21 -> x1, local copies, waits for them, and re-layouts: 6.83 us -> 1.67 us
    pallas_call x1, Pallas kernels: 112 us -> 109 us  [shards(): pl.pallas_call(whole_kernel, out_shape=jax.ShapeDtypeStruct((64, D), BF),...]
    reshape x5 -> x0, local copies, waits for them, and re-layouts: 2.99 us -> none  [shards(): row = lambda v: v.reshape(1, -1)]
where the time goes in v3:
time: 111 us
  Pallas kernels  109 us (98%)
  local copies, waits for them, and re-layouts  1.67 us (2%)
    pallas_call x1, Pallas kernels, shards(): pl.pallas_call(whole_kernel, out_shape=jax.ShapeDtypeStruct((64, D), BF),...  109 us

profile of v3, /device:TPU:1, one launch (start us, length us, event | category | flops | bytes accessed | tf_op | source)
XLA Modules:
  0.0 111.0 jit_solution(13575388890366380128)
XLA Ops:
  0.7 108.7 %whole.1 = bf16[64,2048]{1,0:T(8,128)(2,1)} custom-call(bf16[64,2048]{1,0:T(8,128)(2,1)} %lat_ref.1, bf16[32,2048]{1,0:T(8,128)(2,1)} %context_ref.1, bf16[16,128]{1,0:T(8,128)(2,1)} %bitcast.17, bf16[16,128]{1,0:T(8,128)(2,1)} %bitcast.18, bf16[3,128,128]{2,1,0:T(8,128)(2,1)} %mw_ref.1, bf16[16,128]{1,0:T(8,128)(2,1)} %bitcast.19, bf16[128,768]{1,0:T(8,128)(2,1)} %dq_ref.1, ...), custom_call_target="tpu_custom_call" | custom-call | tf_op jit(solution)/shard_map/whole/pallas_call | solution.py:685
  109.3 1.7 %copy.23 = bf16[64,2048]{1,0:T(8,128)(2,1)} copy(bf16[64,2048]{1,0:T(8,128)(2,1)} %whole.1) | data formatting | bytes 524288

commit v4 on v3

--- a/solution.py
+++ b/solution.py
@@ -160,6 +160,45 @@
             device_id_type=pl.DeviceIdType.MESH).wait_send()
 
 
+CHIPS = (1, -1, 2, -2, 3, -3, 4)
+
+
+class PlaneShare:
+    def __init__(self, board, place, bufs):
+        self.board, self.place, self.bufs = board, place, bufs
+        self.base = board.take(len(CHIPS) * 4)
+
+    def rows(self, part, offset):
+        at = ((self.place.x, self.place.y)[part] + offset + 4) % 4 * 32
+        return pl.ds(pl.multiple_of(at, 32), 32)
+
+    def view(self, dist, part, offset):
+        return self.bufs[part].at[(self.place.z - dist + 16) % 8, self.rows(part, offset)]
+
+    def number(self, dist, part, kind):
+        return self.base + (CHIPS.index(dist) * 2 + part) * 2 + kind
+
+    def device(self, part, step):
+        return self.place.plane(("x", "y")[part], step)
+
+    def send(self, dist, part):
+        own = self.view(dist, part, 0)
+        self.board.send(self.number(dist, part, 0), own, own, self.device(part, 1))
+        self.board.send(self.number(dist, part, 1), own, own, self.device(part, -1))
+
+    def arrived(self, dist, part):
+        for kind, step in ((0, 1), (1, -1)):
+            self.board.arrived(self.number(dist, part, kind), self.view(dist, part, -step),
+                               self.device(part, -step))
+
+    def drain(self):
+        for dist in CHIPS:
+            for part in (0, 1):
+                for kind, step in ((0, 1), (1, -1)):
+                    self.board.sent(self.number(dist, part, kind), self.view(dist, part, 0),
+                                    self.device(part, step))
+
+
 class Place:
     def __init__(self):
         self.s = lax.axis_index("sp")
@@ -197,7 +236,8 @@
 
 
 class ZRing:
-    def __init__(self, board, place, own, bufs, by_device=False):
+    def __init__(self, board, place, own, bufs, by_device=False, rows=None):
+        self.rows = rows
         self.board, self.place, self.own, self.bufs = board, place, own, bufs
         self.by_device = by_device
         self.base = board.take(16)
@@ -206,7 +246,12 @@
         return self.base + (0 if way == 1 else 8) + (dist - 1) * 2 + part
 
     def slot(self, way, dist, part):
-        return self.bufs[part].at[self.index(way * dist)]
+        return self.view(part, way * dist)
+
+    def view(self, part, back):
+        if self.rows is None:
+            return self.bufs[part].at[self.index(back)]
+        return self.bufs[part].at[self.index(back), self.rows[part]]
 
     def index(self, back):
         at = (self.place.z - back + 16) % 8
@@ -219,7 +264,7 @@
     def begin_part(self, part):
         for way in (1, -1):
             self.board.send(self.number(way, 1, part), self.own[part],
-                            self.bufs[part].at[self.index(0)], self.place.ring(way))
+                            self.view(part, 0), self.place.ring(way))
 
     def take(self, way, dist, part):
         here = self.slot(way, dist, part)
@@ -272,7 +317,13 @@
     share_base = board.take(16)
     half_cols = D // 2
     ring = ZRing(board, place, (ow_ref.at[:, :half_cols], ow_ref.at[:, half_cols:]), (owa, owb))
-    wring = ZRing(board, place, (dq_ref, dkv_ref), (wq, wkv))
+    share_w = PlaneShare(board, place, (wq, wkv))
+    quarter = (share_w.rows(0, 0), share_w.rows(1, 0))
+    wring = ZRing(board, place, (dq_ref.at[quarter[0]], dkv_ref.at[quarter[1]]), (wq, wkv),
+                  rows=quarter)
+    facing = (share_w.rows(0, 2), share_w.rows(1, 2))
+    oring = ZRing(board, place, (dq_ref.at[facing[0]], dkv_ref.at[facing[1]]), (wq, wkv),
+                  rows=facing)
     lring = ZRing(board, place, (lk.at[place.t], lq.at[place.t]), (lk, lq), by_device=True)
 
     mark("a_greet")
@@ -280,6 +331,7 @@
 
     mark("b_mod")
     wring.begin()
+    oring.begin()
     board.send(lat_d2d, lat_ref, latsib, place.sibling())
 
     def silu(ref):
@@ -317,6 +369,23 @@
     inv_ctx = inverse(context_ref)
 
     mark("d_modwait")
+    def from_ring(dist):
+        for part in (0, 1):
+            if dist == 4:
+                wring.take(1 if part == 0 else -1, 4, part)
+                share_w.send(4, part)
+                continue
+            for way in (1, -1):
+                wring.take(way, dist, part)
+                share_w.send(way * dist, part)
+
+    def facing_ring(dist):
+        for part in (0, 1):
+            for way in ((1 if part == 0 else -1,) if dist == 4 else (1, -1)):
+                oring.take(way, dist, part)
+
+    from_ring(1)
+    facing_ring(1)
     for k in range(1, 16):
         board.arrived(modp_base + k, modp.at[(place.s - k + 16) % 16], place.sp_peer(16 - k))
     modf[place.t] = jnp.sum(modp[...], axis=0)
@@ -325,9 +394,8 @@
 
     board.arrived(lat_d2d, latsib, place.sibling())
     inv_sib = inverse(latsib)
-    w_items = wring.items()
-    for item in w_items[:4]:
-        wring.take(*item)
+    from_ring(2)
+    facing_ring(2)
     mark("e_modfwait")
     for k in range(1, 16):
         board.arrived(modf_base + k, modf.at[(place.t - k + 16) % 16], place.tp_peer(16 - k))
@@ -361,10 +429,20 @@
                                       preferred_element_type=F32)
     rope = rope.astype(BF).astype(F32)
     mark("g_wring")
-    for n, (way, dist, part) in enumerate(w_items):
-        if n >= 4:
-            wring.take(way, dist, part)
-        add_product(wring.index(way * dist), part)
+    def finish_chip(dist):
+        for part in (0, 1):
+            for d in ((4,) if dist == 4 else (dist, -dist)):
+                share_w.arrived(d, part)
+                add_product((place.z - d + 16) % 8, part)
+
+    from_ring(3)
+    finish_chip(1)
+    facing_ring(3)
+    finish_chip(2)
+    from_ring(4)
+    finish_chip(3)
+    facing_ring(4)
+    finish_chip(4)
 
     mark("h_d2dpart")
     board.send(part_base + 1, ukv.at[64:160], skv, place.sibling())
@@ -426,6 +504,8 @@
 
     def finish():
         wring.drain()
+        oring.drain()
+        share_w.drain()
         lring.drain()
         board.sent(lat_d2d, lat_ref, place.sibling())
         for k in range(1, 16):
@@ -678,7 +758,7 @@
 ):
     vmem = pl.BlockSpec(memory_space=pltpu.VMEM)
     smem = pl.BlockSpec(memory_space=pltpu.SMEM)
-    copies = len(ITEM_ORDER) + 16 + 8 + 2 + 32 + 2 + 16 + 3 * 16
+    copies = len(ITEM_ORDER) + 16 + 8 + 2 + 32 + 2 + 16 + 4 * 16 + 28
     base, table = rotation_tables()
     row = lambda v: v.reshape(1, -1)
     fold = lambda v: v.reshape(-1, 128)

time: 111 us -> 103 us (0.928)
  Pallas kernels: 109 us -> 101 us
    pallas_call x1, Pallas kernels: 109 us -> 101 us  [shards(): pl.pallas_call(whole_kernel, out_shape=jax.ShapeDtypeStruct((64, D), BF),...]
where the time goes in v4:
time: 103 us
  Pallas kernels  101 us (98%)
  local copies, waits for them, and re-layouts  1.67 us (2%)
    pallas_call x1, Pallas kernels, shards(): pl.pallas_call(whole_kernel, out_shape=jax.ShapeDtypeStruct((64, D), BF),...  101 us

profile of v4, /device:TPU:1, one launch (start us, length us, event | category | flops | bytes accessed | tf_op | source)
XLA Modules:
  0.0 103.4 jit_solution(11083389296855440802)
XLA Ops:
  0.7 101.0 %whole.1 = bf16[64,2048]{1,0:T(8,128)(2,1)} custom-call(bf16[64,2048]{1,0:T(8,128)(2,1)} %lat_ref.1, bf16[32,2048]{1,0:T(8,128)(2,1)} %context_ref.1, bf16[16,128]{1,0:T(8,128)(2,1)} %bitcast.17, bf16[16,128]{1,0:T(8,128)(2,1)} %bitcast.18, bf16[3,128,128]{2,1,0:T(8,128)(2,1)} %mw_ref.1, bf16[16,128]{1,0:T(8,128)(2,1)} %bitcast.19, bf16[128,768]{1,0:T(8,128)(2,1)} %dq_ref.1, ...), custom_call_target="tpu_custom_call" | custom-call | tf_op jit(solution)/shard_map/whole/pallas_call | solution.py:765
  101.7 1.7 %copy.23 = bf16[64,2048]{1,0:T(8,128)(2,1)} copy(bf16[64,2048]{1,0:T(8,128)(2,1)} %whole.1) | data formatting | bytes 524288

commit v5 on v4

--- a/solution.py
+++ b/solution.py
@@ -29,60 +29,63 @@
 def exchange_items():
     items = {}
     for h in (0, 1):
-        def add(da, db, part, axis, step, trigger):
-            names = ("x", "y") if h == 0 else ("y", "x")
-            items[(h, da, db, part)] = (names[axis], step, trigger)
-        add(-1, 0, "U", 0, 1, None)
-        add(1, 0, "U", 0, -1, None)
-        add(2, 0, 0, 0, 1, (h, -1, 0, "U"))
-        add(2, 0, 1, 0, -1, (h, 1, 0, "U"))
-        for da in (0, -1, 1):
-            trigger = None if da == 0 else (h, da, 0, "U")
-            add(da, -1, "U", 1, 1, trigger)
-            add(da, 1, "U", 1, -1, trigger)
-            add(da, 2, 0, 1, 1, (h, da, -1, "U"))
-            add(da, 2, 1, 1, -1, (h, da, 1, "U"))
         for q in (0, 1):
-            add(2, -1, q, 1, 1, (h, 2, 0, q))
-            add(2, 1, q, 1, -1, (h, 2, 0, q))
-        add(2, 2, 0, 1, 1, (h, 2, -1, 0))
-        add(2, 2, 1, 1, -1, (h, 2, 1, 1))
+            def add(da, db, part, axis, step, trigger):
+                names = ("x", "y") if q == 0 else ("y", "x")
+                trigger = None if trigger is None else (h, q) + trigger
+                items[(h, q, da, db, part)] = (names[axis], step, trigger)
+            add(-1, 0, "U", 0, 1, None)
+            add(1, 0, "U", 0, -1, None)
+            add(2, 0, 0, 0, 1, (-1, 0, "U"))
+            add(2, 0, 1, 0, -1, (1, 0, "U"))
+            for da in (0, -1, 1):
+                trigger = None if da == 0 else (da, 0, "U")
+                add(da, -1, "U", 1, 1, trigger)
+                add(da, 1, "U", 1, -1, trigger)
+                add(da, 2, 0, 1, 1, (da, -1, "U"))
+                add(da, 2, 1, 1, -1, (da, 1, "U"))
+            for part in (0, 1):
+                add(2, -1, part, 1, 1, (2, 0, part))
+                add(2, 1, part, 1, -1, (2, 0, part))
+            add(2, 2, 0, 1, 1, (2, -1, 0))
+            add(2, 2, 1, 1, -1, (2, 1, 1))
     return items
 
 
-RELEASE = (10.0, 17.5)
-EARLY_AT = 16.0
-LOOP_AT = 19.5
-STEP = 0.78
-UNIT, LATENCY = 3.53, 1.9
+def unit_of(key):
+    h, q, da, db, _ = key
+    return (h, da, db) if q == 0 else (h, db, da)
+
+
+RELEASE = (9.0, 17.4)
+LOOKS = (13.2, 16.0, 18.8)
+LOOP_AT = 20.2
+STEP = 0.79
+UNIT, LATENCY = 1.85, 2.0
 
 
 def plan_exchange(items):
     free, arrive = {}, {}
-    left = dict(items)
+    taken = []
 
     def send(key, at):
         axis, step, _ = items[key]
         begin = max(at, free.get((axis, step), 0.0))
-        free[(axis, step)] = begin + (UNIT if key[3] == "U" else UNIT / 2)
+        free[(axis, step)] = begin + (UNIT if key[4] == "U" else UNIT / 2)
         arrive[key] = free[(axis, step)] + LATENCY
 
     def begin_half(h, at):
-        keys = [k for k in items if items[k][2] is None and k[0] == h]
-        first = "x" if h == 0 else "y"
-        for key in sorted(keys, key=lambda k: 0 if items[k][0] == first else 1):
+        for key in own_keys(items, h):
             send(key, at)
 
-    taken = []
-
     def rank(key):
-        return (round(arrive[key], 1), 0 if key[2] == 0 else 1, str(key))
-
-    def take(now, limit=None):
+        return (round(arrive[key], 1), 0 if key[3] == 0 else 1, str(key))
+
+    def take(now):
         got = []
         while True:
             here = sorted((k for k in arrive if k not in taken and arrive[k] <= now), key=rank)
-            if not here or (limit is not None and len(got) >= limit):
+            if not here:
                 return got
             key = here[0]
             taken.append(key)
@@ -92,30 +95,39 @@
                     send(other, now)
 
     begin_half(0, RELEASE[0])
-    early = take(EARLY_AT, 3)
+    early = [take(LOOKS[0]), take(LOOKS[1])]
     begin_half(1, RELEASE[1])
+    early.append(take(LOOKS[2]))
     now = LOOP_AT
     units = [(0, 0, 0), (1, 0, 0)]
-    every = sorted({k[:3] for k in items})
+    every = sorted({unit_of(k) for k in items})
+
+    def come(u):
+        return max(arrive[k] for k in items if unit_of(k) == u)
 
     def ready():
         done = [u for u in every if u not in units
-                and all(k in taken for k in items if k[:3] == u)]
-        return sorted(done, key=lambda u: (max(arrive[k] for k in items if k[:3] == u), str(u)))
+                and all(k in taken for k in items if unit_of(k) == u)]
+        return sorted(done, key=lambda u: (come(u), str(u)))
 
     plan = [take(now)]
     for n in range(1, len(every) + 3, 2):
         got = take(now)
         while len(units) < min(n + 2, len(every) + 2):
-            come = ready()
-            if come:
-                units.append(come[0])
+            found = ready()
+            if found:
+                units.append(found[0])
                 continue
             now = min(arrive[k] for k in arrive if k not in taken)
             got = got + take(now)
         plan.append(got)
         now += 2 * STEP
     return early, plan, units, now
+
+
+def own_keys(items, h):
+    keys = [k for k in items if items[k][2] is None and k[0] == h]
+    return sorted(keys, key=lambda k: 0 if items[k][0] == ("x", "y")[k[1]] else 1)
 
 
 ITEMS = exchange_items()
@@ -292,10 +304,10 @@
                 self.board.sent(self.number(way, dist, part), here, self.place.ring(way))
 
 
-def quarter_ref(buf, slot, part):
+def quarter_ref(buf, slot, quarter, part):
     if part == "U":
-        return buf.at[slot]
-    return buf.at[slot, part]
+        return buf.at[slot, quarter]
+    return buf.at[slot, quarter, :, 128 * part:128 * part + 128]
 
 
 def whole_kernel(lat_ref, context_ref, cond_ref, condc_ref, mw_ref, ng_ref, dq_ref, dkv_ref,
@@ -517,30 +529,23 @@
         for n, part in enumerate(share_sizes):
             board.sent(share_base + n, (lk, lq)[part].at[0], place.sibling())
 
+    def kv_ref(key):
+        return quarter_ref(kvb, SLOT[unit_of(key)], key[1], key[4])
+
     def kv_send(key, src):
         axis, step, _ = ITEMS[key]
-        h, da, db, part = key
-        board.send(kv_base + ITEM_INDEX[key], src, quarter_ref(kvb, SLOT[key[:3]], part),
-                   place.plane(axis, step))
-
-    def own_part(h):
-        return kvb.at[SLOT[(h, 0, 0)]]
+        board.send(kv_base + ITEM_INDEX[key], src, kv_ref(key), place.plane(axis, step))
 
     def kv_begin(h):
-        for key in sorted((k for k in ITEMS if ITEMS[k][2] is None and k[0] == h),
-                          key=lambda k: 0 if ITEMS[k][0] == ("x" if k[0] == 0 else "y") else 1):
-            kv_send(key, own_part(h))
+        for key in own_keys(ITEMS, h):
+            kv_send(key, kvb.at[SLOT[(h, 0, 0)], key[1]])
 
     def kv_take(key):
         axis, step, _ = ITEMS[key]
-        here = quarter_ref(kvb, SLOT[key[:3]], key[3])
-        board.arrived(kv_base + ITEM_INDEX[key], here, place.plane(axis, -step))
+        board.arrived(kv_base + ITEM_INDEX[key], kv_ref(key), place.plane(axis, -step))
         for other in ITEM_ORDER:
             if ITEMS[other][2] == key:
-                src = here
-                if key[3] == "U" and other[3] != "U":
-                    src = kvb.at[SLOT[key[:3]], other[3]]
-                kv_send(other, src)
+                kv_send(other, quarter_ref(kvb, SLOT[unit_of(key)], key[1], other[4]))
 
     mark("j_lring")
     l_items = lring.items()
@@ -596,6 +601,8 @@
     ring_take(-1, 3, 0)
     chip_keys(-2, 1, 0)
     chip_queries(2)
+    for key in EARLY[0]:
+        kv_take(key)
     ring_take(1, 3, 1)
     ring_take(-1, 3, 1)
     ring.begin()
@@ -603,7 +610,7 @@
     chip_keys(-3, 1, 2)
     chip_queries(-2)
     mark("l_early")
-    for key in EARLY:
+    for key in EARLY[1]:
         kv_take(key)
     mark("l_h1")
     ring_take(1, 4, 0)
@@ -612,6 +619,8 @@
     mark("l_q")
     chip_queries(3)
     chip_queries(-3)
+    for key in EARLY[2]:
+        kv_take(key)
     ring_take(-1, 4, 1)
     chip_queries(4)
 
@@ -638,7 +647,11 @@
                 top = jnp.max(scores, axis=0, keepdims=True)
                 mb_ref[:, cols] = top if q == 0 else jnp.maximum(mb_ref[:, cols], top)
 
+    ones = jnp.ones((16, 256), BF)
+
     def absorb(slot, s_ref, mb_ref, bias):
+        values = [jnp.concatenate([kvb[slot, q, HEAD:HEAD + VDIM, :], ones], axis=0)
+                  for q in (0, 1)]
         for n in range(4):
             cols = slice(n * 256, (n + 1) * 256)
             old = m_ref[:, cols]
@@ -650,18 +663,16 @@
             factor = jnp.exp2(old - new)
             less = new if bias is None else new - bias
             weights = jnp.exp2(s_ref[:, cols] * SCALE2 - less)
-            l_ref[:, cols] = l_ref[:, cols] * factor + jnp.sum(weights, axis=0, keepdims=True)
             rounded = weights.astype(BF)
-            summed = jnp.dot(kvb[slot, 0, HEAD:HEAD + VDIM, :], rounded[:256],
-                             preferred_element_type=F32)
-            summed = summed + jnp.dot(kvb[slot, 1, HEAD:HEAD + VDIM, :], rounded[256:],
-                                      preferred_element_type=F32)
-            acc[:, cols] = acc[:, cols] * factor + summed
+            summed = jnp.dot(values[0], rounded[:256], preferred_element_type=F32)
+            summed = summed + jnp.dot(values[1], rounded[256:], preferred_element_type=F32)
+            l_ref[:, cols] = l_ref[:, cols] * factor + summed[VDIM:VDIM + 1]
+            acc[:, cols] = acc[:, cols] * factor + summed[:VDIM]
 
     ring_items = ring.items()
     ring_plan = [[] for _ in range(17)]
     for n, item in enumerate(ring_items):
-        ring_plan[min(2 + (n * 13) // len(ring_items), 16)].append(item)
+        ring_plan[16 if n >= 12 else 1 + n].append(item)
 
     def actions(n):
         for key in PLAN[n]:
@@ -719,7 +730,7 @@
     finish()
     for key in ITEM_ORDER:
         axis, step, _ = ITEMS[key]
-        src = quarter_ref(kvb, 0, key[3])
+        src = quarter_ref(kvb, 0, 0, key[4])
         board.sent(kv_base + ITEM_INDEX[key], src, place.plane(axis, step))
     mark(None)
 

time: 103 us -> 97.4 us (0.946)
  Pallas kernels: 101 us -> 95 us
    pallas_call x1, Pallas kernels: 101 us -> 95 us  [shards(): pl.pallas_call(whole_kernel, out_shape=jax.ShapeDtypeStruct((64, D), BF),...]
where the time goes in v5:
time: 97.4 us; the launch traced here: 97.3 us
  Pallas kernels  95 us (98%)
  local copies, waits for them, and re-layouts  1.67 us (2%)
    pallas_call x1, Pallas kernels, shards(): pl.pallas_call(whole_kernel, out_shape=jax.ShapeDtypeStruct((64, D), BF),...  95 us

profile of v5, /device:TPU:1, one launch (start us, length us, event | category | flops | bytes accessed | tf_op | source)
XLA Modules:
  0.0 97.3 jit_solution(3228271715866572845)
XLA Ops:
  0.7 95.0 %whole.1 = bf16[64,2048]{1,0:T(8,128)(2,1)} custom-call(bf16[64,2048]{1,0:T(8,128)(2,1)} %lat_ref.1, bf16[32,2048]{1,0:T(8,128)(2,1)} %context_ref.1, bf16[16,128]{1,0:T(8,128)(2,1)} %bitcast.17, bf16[16,128]{1,0:T(8,128)(2,1)} %bitcast.18, bf16[3,128,128]{2,1,0:T(8,128)(2,1)} %mw_ref.1, bf16[16,128]{1,0:T(8,128)(2,1)} %bitcast.19, bf16[128,768]{1,0:T(8,128)(2,1)} %dq_ref.1, ...), custom_call_target="tpu_custom_call" | custom-call | tf_op jit(solution)/shard_map/whole/pallas_call | solution.py:776
  95.6 1.7 %copy.23 = bf16[64,2048]{1,0:T(8,128)(2,1)} copy(bf16[64,2048]{1,0:T(8,128)(2,1)} %whole.1) | data formatting | bytes 524288

commit v6 on v5

--- a/solution.py
+++ b/solution.py
@@ -321,7 +321,7 @@
     kv_base = board.take(len(ITEM_ORDER))
     ctx_base = board.take(16)
     a2a_base = board.take(8)
-    d2d = board.take(1)
+    d2d = board.take(2)
     lat_d2d = board.take(1)
     modp_base = board.take(16)
     modf_base = board.take(16)
@@ -408,6 +408,8 @@
     inv_sib = inverse(latsib)
     from_ring(2)
     facing_ring(2)
+    from_ring(3)
+    facing_ring(3)
     mark("e_modfwait")
     for k in range(1, 16):
         board.arrived(modf_base + k, modf.at[(place.t - k + 16) % 16], place.tp_peer(16 - k))
@@ -447,11 +449,9 @@
                 share_w.arrived(d, part)
                 add_product((place.z - d + 16) % 8, part)
 
-    from_ring(3)
     finish_chip(1)
-    facing_ring(3)
+    from_ring(4)
     finish_chip(2)
-    from_ring(4)
     finish_chip(3)
     facing_ring(4)
     finish_chip(4)
@@ -701,27 +701,30 @@
     for k in range(8):
         cols = slice(k * 128, (k + 1) * 128)
         att[k] = (acc[:, cols] / l_ref[:, cols]).astype(BF)
-    for k in range(1, 8):
+    for k in (4, 3, 5, 2, 6, 1, 7):
         board.send(a2a_base + k, att.at[(place.z + k) % 8], attb.at[place.z], place.ring(k))
     attb[place.z] = att[place.z]
     for k in range(1, 8):
         board.arrived(a2a_base + k, attb.at[(place.z - k + 8) % 8], place.ring(-k))
     mark("r_out")
     rows = attb[...].reshape(8 * VDIM, 128).astype(F32).T.astype(BF)
+    away_rows = pl.ds(pl.multiple_of(64 * (1 - place.c), 64), 64)
     for n, weight in enumerate((owa, owb)):
-        part_ref[:, n * half_cols:(n + 1) * half_cols] = jnp.dot(
-            rows, weight[...].reshape(8 * VDIM, half_cols), preferred_element_type=F32)
-    away = part_ref.at[pl.ds(pl.multiple_of(64 * (1 - place.c), 64), 64)]
+        part_ref[n] = jnp.dot(rows, weight[...].reshape(8 * VDIM, half_cols),
+                              preferred_element_type=F32)
+        board.send(d2d + n, part_ref.at[n, away_rows], sib_ref.at[n], place.sibling())
     mark("s_d2d")
-    board.send(d2d, away, sib_ref, place.sibling())
-    board.arrived(d2d, sib_ref, place.sibling())
-    gates = jnp.concatenate([modf[k, 2:3, :] for k in range(16)], axis=1)
-    mine = part_ref[pl.ds(pl.multiple_of(64 * place.c, 64), 64)]
-    projected = mine + sib_ref[...]
-    out_ref[...] = (lat_ref[...].astype(F32) + gates * projected).astype(BF)
+    for n in (0, 1):
+        cols = slice(n * half_cols, (n + 1) * half_cols)
+        gates = jnp.concatenate([modf[k, 2:3, :] for k in range(8 * n, 8 * n + 8)], axis=1)
+        mine = part_ref[n, pl.ds(pl.multiple_of(64 * place.c, 64), 64)]
+        board.arrived(d2d + n, sib_ref.at[n], place.sibling())
+        out_ref[:, cols] = (lat_ref[:, cols].astype(F32)
+                            + gates * (mine + sib_ref[n])).astype(BF)
 
     mark("t_drain")
-    board.sent(d2d, away, place.sibling())
+    for n in (0, 1):
+        board.sent(d2d + n, sib_ref.at[n], place.sibling())
     for k in range(1, 8):
         board.sent(a2a_base + k, att.at[(place.z + k) % 8], place.ring(k))
     for k in range(1, 16):
@@ -769,7 +772,7 @@
 ):
     vmem = pl.BlockSpec(memory_space=pltpu.VMEM)
     smem = pl.BlockSpec(memory_space=pltpu.SMEM)
-    copies = len(ITEM_ORDER) + 16 + 8 + 2 + 32 + 2 + 16 + 4 * 16 + 28
+    copies = len(ITEM_ORDER) + 16 + 8 + 3 + 32 + 2 + 16 + 4 * 16 + 28
     base, table = rotation_tables()
     row = lambda v: v.reshape(1, -1)
     fold = lambda v: v.reshape(-1, 128)
@@ -807,8 +810,8 @@
             pltpu.VMEM((VDIM, 1024), F32),
             pltpu.VMEM((8, VDIM, 128), BF),
             pltpu.VMEM((8, VDIM, 128), BF),
-            pltpu.VMEM((128, D), F32),
-            pltpu.VMEM((64, D), F32),
+            pltpu.VMEM((2, 128, D // 2), F32),
+            pltpu.VMEM((2, 64, D // 2), F32),
             pltpu.SemaphoreType.DMA((copies,)),
             pltpu.SemaphoreType.DMA((copies,)),
         ],

time: 97.4 us -> 96.7 us (level)
  no operation moved by 1% of the time
where the time goes in v6:
time: 96.7 us; the launch traced here: 96.5 us
  Pallas kernels  94.2 us (97%)
  local copies, waits for them, and re-layouts  1.67 us (2%)
    pallas_call x1, Pallas kernels, shards(): pl.pallas_call(whole_kernel, out_shape=jax.ShapeDtypeStruct((64, D), BF),...  94.2 us

profile of v6, /device:TPU:1, one launch (start us, length us, event | category | flops | bytes accessed | tf_op | source)
XLA Modules:
  0.0 96.5 jit_solution(5694128162520242439)
XLA Ops:
  0.7 94.2 %whole.1 = bf16[64,2048]{1,0:T(8,128)(2,1)} custom-call(bf16[64,2048]{1,0:T(8,128)(2,1)} %lat_ref.1, bf16[32,2048]{1,0:T(8,128)(2,1)} %context_ref.1, bf16[16,128]{1,0:T(8,128)(2,1)} %bitcast.17, bf16[16,128]{1,0:T(8,128)(2,1)} %bitcast.18, bf16[3,128,128]{2,1,0:T(8,128)(2,1)} %mw_ref.1, bf16[16,128]{1,0:T(8,128)(2,1)} %bitcast.19, bf16[128,768]{1,0:T(8,128)(2,1)} %dq_ref.1, ...), custom_call_target="tpu_custom_call" | custom-call | tf_op jit(solution)/shard_map/whole/pallas_call | solution.py:779
  94.9 1.7 %copy.23 = bf16[64,2048]{1,0:T(8,128)(2,1)} copy(bf16[64,2048]{1,0:T(8,128)(2,1)} %whole.1) | data formatting | bytes 524288
